TPU v7x, 32 devices: a whole 2x2x4 slice. The times are simulated.
32 devices in a mesh: grp: 2 (over y), ep: 4 (over z), tp: 4 (over x, core).
Axes of the slice: x: 2, y: 2, z: 4, core: 2. Of those that a mesh axis runs over, the one named last changes fastest.
Arguments:
- mixer_tokens: bfloat16 [4096, 2048], P(('grp', 'ep', 'tp')), parts along dimension 0, may hold values from -6 to 6
- mixer_gain: bfloat16 [2048], replicated, may hold values from 0.099609375 to 1.8984375
- in_weight: bfloat16 [2048, 2048], P(None, 'tp'), may hold values from -0.125 to 0.125
- group_weight: bfloat16 [4, 512, 512], P('tp'), may hold values from -0.25 to 0.25
- channel_scale: bfloat16 [2048], P('tp'), may hold values from 0.099609375 to 1.8984375
- out_weight: bfloat16 [2048, 2048], P('tp'), may hold values from -0.125 to 0.125
- expert_tokens: bfloat16 [4096, 2048], P(('grp', 'ep', 'tp')), parts along dimension 0, may hold values from -6 to 6
- expert_gain: bfloat16 [2048], replicated, may hold values from 0.099609375 to 1.8984375
- route_ids: int32 [4096, 2], P(('grp', 'ep', 'tp')), parts along dimension 0, may hold values from 0 to 3, all different within a row; in each aligned block of 128 rows (0 to 127, 128 to 255, ...) at most 128 rows name the same one
- route_weights: float32 [4096, 2], P(('grp', 'ep', 'tp')), parts along dimension 0, may hold values from 0.1 to 1
- gate_weight: bfloat16 [4, 2048, 1024], P('ep', None, 'tp'), may hold values from -0.125 to 0.125
- up_weight: bfloat16 [4, 2048, 1024], P('ep', None, 'tp'), may hold values from -0.125 to 0.125
- down_weight: bfloat16 [4, 1024, 2048], P('ep', 'tp'), may hold values from -0.1875 to 0.1875
Outputs:
- mixed_tokens: bfloat16 [4096, 2048], P(('grp', 'ep', 'tp')), parts along dimension 0
- expert_mix: bfloat16 [4096, 2048], P(('grp', 'ep', 'tp')), parts along dimension 0
There are 2 independent parts, one for each index of `grp`. A program takes and returns all parts, laid end to end along the dimension named above; an argument that names none is the same for every part. Nothing has to cross between parts.
Inputs may be any that keep to these rules, and one draw needn't show every extreme that they name: `route_ids`: each row names 2 different experts; in the rows of one device no expert is named more than 128 times, and one expert exactly 128 times in the rows of some device.
All inputs are finite; a program needn't handle non-finite values.
Results may differ from a plain program's by a relative error of at most 0.015.
Values may be sent and summed in bfloat16 or wider, within the bound.
A program may use at most 128 MiB of HBM per device.

v0:
```python
import jax
import jax.numpy as jnp
from jax import lax
from jax.sharding import PartitionSpec as P

WINDOW_MAX = 16


def shifted(value, axis, by):
    devices = lax.axis_size(axis)
    pairs = [(i, i + by) for i in range(devices) if 0 <= i + by < devices]
    return lax.ppermute(value, axis, pairs)


def turned(value, axis, by):
    devices = lax.axis_size(axis)
    if by % devices == 0:
        return value
    return lax.ppermute(value, axis, [(i, (i + by) % devices) for i in range(devices)])


def rms_rows(rows, gain):
    values = rows.astype(jnp.float32)
    scaled = values * lax.rsqrt(jnp.mean(values * values, axis=-1, keepdims=True) + 1e-06)
    return (scaled * gain.astype(jnp.float32)).astype(jnp.bfloat16)


def expert_hidden(rows, w_gate, w_up):
    gate = jnp.dot(rows, w_gate, preferred_element_type=jnp.float32)
    upper = jnp.dot(rows, w_up, preferred_element_type=jnp.float32)
    return (jax.nn.silu(gate) * upper).astype(jnp.bfloat16)


def local(
    mixer_tokens,
    mixer_gain,
    in_weight,
    group_weight,
    channel_scale,
    out_weight,
    expert_tokens,
    expert_gain,
    route_ids,
    route_weights,
    gate_weight,
    up_weight,
    down_weight,
):
    normed = rms_rows(mixer_tokens, mixer_gain)
    expert_in = rms_rows(expert_tokens, expert_gain)
    shares = route_weights / jnp.sum(route_weights, axis=1, keepdims=True)
    rows_here, top_k = route_ids.shape
    width = expert_in.shape[1]
    n_experts = lax.axis_size("ep") * gate_weight.shape[0]
    capacity = 4 * rows_here // n_experts
    dense = capacity >= rows_here
    parts_tp = lax.axis_size("tp")
    if dense:
        both = lax.all_gather(jnp.concatenate([normed, expert_in], axis=0), "tp", axis=0, tiled=True)
        both = both.reshape(parts_tp, 2, rows_here, width)
        every = both[:, 0].reshape(parts_tp * rows_here, width)
        own = both[:, 1].reshape(parts_tp * rows_here, width)
    else:
        every = lax.all_gather(normed, "tp", axis=0, tiled=True)
    pooled_in = jnp.dot(
        every,
        in_weight,
        preferred_element_type=jnp.float32,
    ).astype(jnp.bfloat16)
    block_rows = pooled_in.shape[0]
    rim_rows = shifted(pooled_in[block_rows - WINDOW_MAX :], "ep", 1)
    values = pooled_in.astype(jnp.float32)
    extended = jnp.concatenate([rim_rows.astype(jnp.float32), values], axis=0)
    window = jnp.left_shift(jnp.int32(2), lax.axis_index("tp"))
    sums = extended
    span = 1
    total = jnp.zeros_like(values)
    for level in range(WINDOW_MAX.bit_length() - 1):
        sums = sums[span:] + sums[:-span]
        span = span * 2
        total = total + jnp.where(window == span, sums[sums.shape[0] - block_rows :], 0.0)
    positions = lax.axis_index("ep") * block_rows + lax.iota(jnp.int32, block_rows) + 1
    counts = jnp.minimum(positions, window).astype(jnp.float32)
    pooled = (total / counts[:, None] - values).astype(jnp.bfloat16)
    grouped = (
        jnp.dot(pooled, group_weight[0], preferred_element_type=jnp.float32)
        * channel_scale.astype(jnp.float32)
    ).astype(jnp.bfloat16)
    mixed_part = jnp.dot(grouped, out_weight, preferred_element_type=jnp.float32).astype(
        jnp.bfloat16
    )
    if dense:
        experts = jnp.arange(n_experts, dtype=jnp.int32)
        named = (route_ids[:, :, None] == experts[None, None, :]).astype(jnp.float32)
        coefs = jnp.sum(named * shares[:, :, None], axis=1)
        coefs = lax.all_gather(coefs, ("ep", "tp"), axis=0, tiled=True)
        blocks = lax.axis_size("ep")
        here = lax.axis_index("ep")
        mine = (experts == here).astype(jnp.float32)
        coef = jnp.sum(coefs * mine[None, :], axis=1).reshape(blocks, parts_tp, rows_here)
        order = list(range(1, blocks))

        def scale_of(k):
            return lax.dynamic_index_in_dim(coef, lax.rem(here - k + blocks, blocks), 0, False)

        def expert_part(rows, scale):
            hidden = expert_hidden(rows, gate_weight[0], up_weight[0])
            part = jnp.dot(hidden, down_weight[0], preferred_element_type=jnp.float32)
            return (part * scale.reshape(-1)[:, None]).astype(jnp.bfloat16)

        moved = jnp.concatenate([turned(expert_in, "ep", k) for k in order], axis=0)
        moved, own = lax.optimization_barrier((moved, own))
        own_part = expert_part(own, scale_of(0))
        others = lax.all_gather(moved, "tp", axis=0, tiled=True)
        part = expert_part(others, jnp.stack([scale_of(k) for k in order], axis=1))
        back = lax.psum_scatter(part, "tp", scatter_dimension=0, tiled=True)
        back = back.reshape(blocks - 1, rows_here, width)
        pair = jnp.stack(
            [value.reshape(parts_tp, rows_here, width) for value in (mixed_part, own_part)], axis=1
        ).reshape(2 * parts_tp * rows_here, width)
        pair = lax.psum_scatter(pair, "tp", scatter_dimension=0, tiled=True)
        total = pair[rows_here:].astype(jnp.float32)
        for i, k in enumerate(order):
            total = total + turned(back[i], "ep", -k).astype(jnp.float32)
        return (pair[:rows_here], total.astype(jnp.bfloat16))
    mixed_tokens = lax.psum_scatter(mixed_part, "tp", scatter_dimension=0, tiled=True)
    flat_ids = route_ids.reshape(rows_here * top_k)
    one_hot = (flat_ids[:, None] == jnp.arange(n_experts, dtype=jnp.int32)[None, :]).astype(
        jnp.int32
    )
    before = jnp.cumsum(one_hot, axis=0) - one_hot
    slots = jnp.sum(before * one_hot, axis=1)
    targets = flat_ids * capacity + slots
    placement = (
        targets.reshape(rows_here, top_k)[None, :, :]
        == jnp.arange(n_experts * capacity, dtype=jnp.int32)[:, None, None]
    )
    dispatch = jnp.any(placement, axis=2).astype(jnp.bfloat16)
    outgoing = jnp.dot(dispatch, expert_in, preferred_element_type=jnp.float32).astype(jnp.bfloat16)
    outgoing = outgoing.reshape(n_experts, capacity, width)
    arrived = lax.all_to_all(outgoing, "ep", split_axis=0, concat_axis=0, tiled=True)
    sources, held, _ = arrived.shape
    flat = arrived.reshape(sources * held, width)
    hidden = expert_hidden(
        lax.all_gather(flat, "tp", axis=0, tiled=True), gate_weight[0], up_weight[0]
    )
    rows = hidden
    summed = lax.psum_scatter(
        jnp.dot(rows, down_weight[0], preferred_element_type=jnp.float32).astype(jnp.bfloat16),
        "tp",
        scatter_dimension=0,
        tiled=True,
    ).astype(jnp.float32)
    expert_out = lax.all_to_all(
        summed.reshape(sources, held, width).astype(jnp.bfloat16),
        "ep",
        split_axis=0,
        concat_axis=0,
        tiled=True,
    ).astype(jnp.float32)
    flat_out = expert_out.reshape(n_experts * capacity, width)
    picked = jnp.take(flat_out, targets, axis=0).reshape(rows_here, top_k, width)
    expert_mix = jnp.sum(picked * shares[:, :, None], axis=1).astype(jnp.bfloat16)
    return (mixed_tokens, expert_mix)


def solution(mesh):
    placed = (
        P(("grp", "ep", "tp"), None),
        P(),
        P(None, "tp"),
        P("tp", None, None),
        P("tp"),
        P("tp", None),
        P(("grp", "ep", "tp"), None),
        P(),
        P(("grp", "ep", "tp"), None),
        P(("grp", "ep", "tp"), None),
        P("ep", None, "tp"),
        P("ep", None, "tp"),
        P("ep", "tp", None),
    )
    return jax.shard_map(
        local,
        mesh=mesh,
        in_specs=placed,
        out_specs=(P(("grp", "ep", "tp"), None), P(("grp", "ep", "tp"), None)),
        check_vma=False,
    )
```

profile of v0, /device:TPU:8, one launch (start us, length us, event | category | flops | bytes accessed | tf_op | source)
XLA Modules:
  0.0 250.2 jit_solution(7683948165691868259)
XLA Ops:
  16.6 1.9 collective-permute-start.3
  18.6 31.7 %collective-permute-done.1 = bf16[128,2048]{1,0:T(8,128)(2,1)S(1)} collective-permute-done((bf16[128,2048]{1,0:T(8,128)(2,1)S(1)}, bf16[128,2048]{1,0:T(8,128)(2,1)S(1)}, u32[]{:S(2)}, u32[]{:S(2)}) %collective-permute-start.1) | collective-permute-done | bytes 524320 | tf_op jit(solution)/shard_map/ppermute | solution.py:19
  50.3 10.1 %collective-permute-done.2 = bf16[128,2048]{1,0:T(8,128)(2,1)S(1)} collective-permute-done((bf16[128,2048]{1,0:T(8,128)(2,1)S(1)}, bf16[128,2048]{1,0:T(8,128)(2,1)S(1)}, u32[]{:S(2)}, u32[]{:S(2)}) %collective-permute-start.2) | collective-permute-done | bytes 524320 | tf_op jit(solution)/shard_map/ppermute | solution.py:19
  60.4 1.8 collective-permute-done.3
  63.5 4.9 %fusion.57 = (bf16[4,1,128,2048]{3,2,1,0:T(8,128)(2,1)}, bf16[4,1,128,2048]{3,2,1,0:T(8,128)(2,1)}) fusion(bf16[4,2,128,2048]{3,2,1,0:T(8,128)(2,1)} %bitcast.41), kind=kLoop, calls=%fused_computation.79 | loop fusion | bytes 8388608 | tf_op jit(solution)/shard_map/slice | solution.py:61
  68.6 18.3 %all_gather.10 = f32[2048,4]{0,1:T(4,128)S(1)} all-gather(f32[128,4]{0,1:T(4,128)S(1)} %select_reduce_fusion), channel_id=1, replica_groups=mesh['grp'=2,'ep'=4,'tp'=4] {'ep','tp'}, dimensions={0}, use_global_device_ids=true | all-gather | bytes 34816 | tf_op jit(solution)/shard_map/all_gather | solution.py:96
  87.0 28.2 %all-gather.5.cloned.1.call-done = bf16[1536,2048]{1,0:T(8,128)(2,1)} async-done(((bf16[384,2048]{1,0:T(8,128)(2,1)}), bf16[1536,2048]{1,0:T(8,128)(2,1)}) %all-gather.5.cloned.1.call-update) | async-done | bytes 6291472 | tf_op jit(solution)/shard_map/all_gather | solution.py:114
  115.2 5.8 %fusion.22 = f32[1536,256]{1,0:T(8,128)} fusion(bf16[1536,2048]{1,0:T(8,128)(2,1)} %all-gather.5.cloned.1.call-done, bf16[1,2048,256]{2,1,0:T(8,128)(2,1)S(1)} %copy-done.8), kind=kOutput, calls=%fused_computation.41 | convolution fusion | flops 1610612736 | bytes 8912896 | tf_op jit(solution)/shard_map/dot_general | solution.py:29
  120.9 11.1 %multiply_convert_fusion = bf16[1536,2048]{1,0:T(8,128)(2,1)} fusion(f32[1536]{0:T(1024)S(1)} %mul.123, bf16[1536,2048]{1,0:T(8,128)(2,1)} %all-gather.5.cloned.1.call-done, f32[1536,256]{1,0:T(8,128)} %fusion.22, bf16[1,256,2048]{2,1,0:T(8,128)(2,1)} %param.25, bf16[1,2048,256]{2,1,0:T(8,128)(2,1)} %param.24), kind=kOutput, calls=%fused_computation | convolution fusion | flops 3229876224 | bytes 16259072 | tf_op jit(solution)/shard_map/dot_general | solution.py:108
  132.7 4.7 %fusion.60 = (f32[512,512]{1,0:T(8,128)}, bf16[512,512]{1,0:T(8,128)(2,1)S(1)}) fusion(bf16[512,2048]{1,0:T(8,128)(2,1)} %bitcast.44, bf16[2048,512]{1,0:T(8,128)(2,1)} %param.15), kind=kOutput, calls=%fused_computation.82 | convolution fusion | flops 1074266112 | bytes 5767168 | tf_op jit(solution)/shard_map/dot_general | solution.py:65
  137.4 3.5 %collective-permute-start = (bf16[16,512]{1,0:T(8,128)(2,1)S(1)}, bf16[16,512]{1,0:T(8,128)(2,1)S(1)}, u32[]{:S(2)}, u32[]{:S(2)}) collective-permute-start(bf16[16,512]{1,0:T(8,128)(2,1)S(1)} %slice.84), channel_id=1, source_target_pairs={{0,4},{4,8},{8,12},{1,5},{5,9},{9,13},{2,6},{6,10},{10,14},{3,7},{... | collective-permute-start | bytes 49160 | tf_op jit(solution)/shard_map/ppermute | solution.py:12
  142.4 6.5 %multiply_convert_fusion.1 = bf16[512,2048]{1,0:T(8,128)(2,1)} fusion(f32[512]{0:T(512)S(1)} %get-tuple-element.16, bf16[512,2048]{1,0:T(8,128)(2,1)} %bitcast.42, bf16[1,256,2048]{2,1,0:T(8,128)(2,1)} %param.25, bf16[1,2048,256]{2,1,0:T(8,128)(2,1)} %param.24, f32[512,256]{1,0:T(8,128)} %fusion.24), kind=kOutput, calls=%fused_computation.2 | convolution fusion | flops 1076625408 | bytes 6817792 | tf_op jit(solution)/shard_map/dot_general | solution.py:108
  149.0 1.9 fusion.3
  152.2 1.7 fusion.59
  153.9 6.4 %convolution_convert_fusion = bf16[512,2048]{1,0:T(8,128)(2,1)} fusion(bf16[512,2048]{1,0:T(8,128)(2,1)S(1)} %copy-done, f32[513,512]{1,0:T(8,128)} %get-tuple-element.12, f32[513,512]{1,0:T(8,128)} %get-tuple-element.11, f32[521,512]{1,0:T(8,128)} %copy-done.2, f32[525,512]{1,0:T(8,128)} %copy-done.1, f32[527,512]{1,0:T(8,128)S(1)} %fusion.3, ...), kind=kOutput, calls=%fused_computation.3 | convolution fusion | flops 1346895872 | bytes 10489860 | tf_op jit(solution)/shard_map/dot_general | solution.py:89
  160.3 2.6 %pad_maximum_fusion = bf16[4,2,128,2048]{3,2,0,1:T(8,128)(2,1)S(1)} fusion(bf16[4,1,128,2048]{3,2,0,1:T(8,128)(2,1)} %bitcast.45, bf16[4,1,128,2048]{3,2,0,1:T(8,128)(2,1)} %bitcast.46), kind=kLoop, calls=%fused_computation.1 | loop fusion | flops 2097152 | bytes 8388608 | tf_op jit(solution)/shard_map/stack | solution.py:118
  162.9 2.3 copy.21
  165.3 25.8 %reduce-scatter.5.cloned.1.call-done = bf16[384,2048]{1,0:T(8,128)(2,1)} async-done(((bf16[1536,2048]{1,0:T(8,128)(2,1)}), bf16[384,2048]{1,0:T(8,128)(2,1)}) %reduce-scatter.5.cloned.1.call-update) | async-done | bytes 1572880 | tf_op jit(solution)/shard_map/reduce_scatter | solution.py:116
  191.1 2.6 %fusion.58 = (bf16[128,2048]{1,0:T(8,128)(2,1)}, bf16[128,2048]{1,0:T(8,128)(2,1)}, bf16[128,2048]{1,0:T(8,128)(2,1)}) fusion(bf16[384,2048]{1,0:T(8,128)(2,1)} %reduce-scatter.5.cloned.1.call-done), kind=kLoop, calls=%fused_computation.80 | loop fusion | bytes 3145728 | tf_op jit(solution)/shard_map/slice | solution.py:124
  194.1 2.4 collective-permute-start.5
  196.6 2.4 collective-permute-start.6
  198.9 39.1 %reduce-scatter.3.cloned.1.call-done = bf16[256,2048]{1,0:T(8,128)(2,1)} async-done(((bf16[1024,2048]{1,0:T(8,128)(2,1)}), bf16[256,2048]{1,0:T(8,128)(2,1)}) %reduce-scatter.3.cloned.1.call-update) | async-done | bytes 1048592 | tf_op jit(solution)/shard_map/reduce_scatter | solution.py:121
  238.1 1.9 slice.99
  241.4 2.3 add_convert_fusion
  (60 shorter events, 16.4 us)
Async XLA Ops:
  7.2 146.7 %copy-start = (bf16[512,2048]{1,0:T(8,128)(2,1)S(1)}, bf16[512,2048]{1,0:T(8,128)(2,1)}, u32[]{:S(2)}) copy-start(bf16[512,2048]{1,0:T(8,128)(2,1)} %param.18) | copy-start | bytes 6291460
  7.2 56.3 %all-gather.3.cloned.1.call-start = ((), (), s32[]{:S(2)}) async-start(), calls=%async_computation.2 | async-start | bytes 5242880 | tf_op jit(solution)/shard_map/all_gather | solution.py:59
  13.8 101.3 %all-gather.5.cloned.1.call-start = ((), (), s32[]{:S(2)}) async-start(), calls=%async_computation.4 | async-start | bytes 7864320 | tf_op jit(solution)/shard_map/all_gather | solution.py:114
  13.9 36.4 %collective-permute-start.1 = (bf16[128,2048]{1,0:T(8,128)(2,1)S(1)}, bf16[128,2048]{1,0:T(8,128)(2,1)S(1)}, u32[]{:S(2)}, u32[]{:S(2)}) collective-permute-start(bf16[128,2048]{1,0:T(8,128)(2,1)S(1)} %get-tuple-element.20), channel_id=1, source_target_pairs={{0,4},{4,8},{8,12},{12,0},{1,5},{5,9},{9,13},{13,1},{2,6},{6,10},{... | collective-permute-start | bytes 1572872 | tf_op jit(solution)/shard_map/ppermute | solution.py:19
  15.5 44.9 %collective-permute-start.2 = (bf16[128,2048]{1,0:T(8,128)(2,1)S(1)}, bf16[128,2048]{1,0:T(8,128)(2,1)S(1)}, u32[]{:S(2)}, u32[]{:S(2)}) collective-permute-start(bf16[128,2048]{1,0:T(8,128)(2,1)S(1)} %get-tuple-element.20), channel_id=1, source_target_pairs={{0,8},{4,12},{8,0},{12,4},{1,9},{5,13},{9,1},{13,5},{2,10},{6,14},... | collective-permute-start | bytes 1572872 | tf_op jit(solution)/shard_map/ppermute | solution.py:19
  16.6 45.6 %collective-permute-start.3 = (bf16[128,2048]{1,0:T(8,128)(2,1)S(1)}, bf16[128,2048]{1,0:T(8,128)(2,1)S(1)}, u32[]{:S(2)}, u32[]{:S(2)}) collective-permute-start(bf16[128,2048]{1,0:T(8,128)(2,1)S(1)} %get-tuple-element.20), channel_id=1, source_target_pairs={{0,12},{4,0},{8,4},{12,8},{1,13},{5,1},{9,5},{13,9},{2,14},{6,2},{... | collective-permute-start | bytes 1572872 | tf_op jit(solution)/shard_map/ppermute | solution.py:19
  63.5 5.0 %copy-start.4 = (f32[128,2]{0,1:T(2,128)S(1)}, f32[128,2]{0,1:T(2,128)}, u32[]{:S(2)}) copy-start(f32[128,2]{0,1:T(2,128)} %param.22) | copy-start | bytes 3076
  63.5 5.0 %copy-start.6 = (s32[128,2]{0,1:T(2,128)S(1)}, s32[128,2]{0,1:T(2,128)}, u32[]{:S(2)}) copy-start(s32[128,2]{0,1:T(2,128)} %param.21) | copy-start | bytes 3076
  63.5 51.7 %copy-start.8 = (bf16[1,2048,256]{2,1,0:T(8,128)(2,1)S(1)}, bf16[1,2048,256]{2,1,0:T(8,128)(2,1)}, u32[]{:S(2)}) copy-start(bf16[1,2048,256]{2,1,0:T(8,128)(2,1)} %param.23) | copy-start | bytes 3145732
  68.4 122.7 %reduce-scatter.5.cloned.1.call-start = ((), (), s32[]{:S(2)}) async-start(), calls=%async_computation.5 | async-start | bytes 7864320 | tf_op jit(solution)/shard_map/reduce_scatter | solution.py:116
  132.0 0.7 copy-start.5
  132.0 106.0 %reduce-scatter.3.cloned.1.call-start = ((), (), s32[]{:S(2)}) async-start(), calls=%async_computation.3 | async-start | bytes 5242880 | tf_op jit(solution)/shard_map/reduce_scatter | solution.py:121
  132.7 8.2 %copy-start.3 = (bf16[4,1,128,2048]{3,2,1,0:T(8,128)(2,1)S(1)}, bf16[4,1,128,2048]{3,2,1,0:T(8,128)(2,1)}, u32[]{:S(2)}) copy-start(bf16[4,1,128,2048]{3,2,1,0:T(8,128)(2,1)} %get-tuple-element.7) | copy-start | bytes 6291460
  132.7 8.2 %copy-start.9 = (bf16[1,2048,256]{2,1,0:T(8,128)(2,1)S(1)}, bf16[1,2048,256]{2,1,0:T(8,128)(2,1)}, u32[]{:S(2)}) copy-start(bf16[1,2048,256]{2,1,0:T(8,128)(2,1)} %param.23) | copy-start | bytes 3145732
  137.4 11.6 %copy-start.7 = (bf16[512,512]{1,0:T(8,128)(2,1)}, bf16[512,512]{1,0:T(8,128)(2,1)S(1)}, u32[]{:S(2)}) copy-start(bf16[512,512]{1,0:T(8,128)(2,1)S(1)} %get-tuple-element.18) | copy-start | bytes 1572868
  137.4 11.6 %collective-permute-start = (bf16[16,512]{1,0:T(8,128)(2,1)S(1)}, bf16[16,512]{1,0:T(8,128)(2,1)S(1)}, u32[]{:S(2)}, u32[]{:S(2)}) collective-permute-start(bf16[16,512]{1,0:T(8,128)(2,1)S(1)} %slice.84), channel_id=1, source_target_pairs={{0,4},{4,8},{8,12},{1,5},{5,9},{9,13},{2,6},{6,10},{10,14},{3,7},{... | collective-permute-start | bytes 49160 | tf_op jit(solution)/shard_map/ppermute | solution.py:12
  151.0 1.0 copy-start.1
  152.2 1.7 copy-start.2
  193.6 46.3 %collective-permute-start.4 = (bf16[128,2048]{1,0:T(8,128)(2,1)}, bf16[128,2048]{1,0:T(8,128)(2,1)S(1)}, u32[]{:S(2)}, u32[]{:S(2)}) collective-permute-start(bf16[128,2048]{1,0:T(8,128)(2,1)} %get-tuple-element.8), channel_id=1, source_target_pairs={{0,12},{4,0},{8,4},{12,8},{1,13},{5,1},{9,5},{13,9},{2,14},{6,2},{... | collective-permute-start | bytes 1572872 | tf_op jit(solution)/shard_map/ppermute | solution.py:19
  194.1 45.8 %collective-permute-start.5 = (bf16[128,2048]{1,0:T(8,128)(2,1)}, bf16[128,2048]{1,0:T(8,128)(2,1)S(1)}, u32[]{:S(2)}, u32[]{:S(2)}) collective-permute-start(bf16[128,2048]{1,0:T(8,128)(2,1)} %get-tuple-element.10), channel_id=1, source_target_pairs={{0,8},{4,12},{8,0},{12,4},{1,9},{5,13},{9,1},{13,5},{2,10},{6,14},... | collective-permute-start | bytes 1572872 | tf_op jit(solution)/shard_map/ppermute | solution.py:19
  196.6 44.8 %collective-permute-start.6 = (bf16[128,2048]{1,0:T(8,128)(2,1)}, bf16[128,2048]{1,0:T(8,128)(2,1)}, u32[]{:S(2)}, u32[]{:S(2)}) collective-permute-start(bf16[128,2048]{1,0:T(8,128)(2,1)} %get-tuple-element.9), channel_id=1, source_target_pairs={{0,4},{4,8},{8,12},{12,0},{1,5},{5,9},{9,13},{13,1},{2,6},{6,10},{... | collective-permute-start | bytes 1572872 | tf_op jit(solution)/shard_map/ppermute | solution.py:19
Sparse Core Ops, SparseCore 0:
  14.0 35.5 all-gather.2
  68.5 46.5 all-gather.4
  132.1 58.8 reduce-scatter.4
  193.5 44.5 reduce-scatter.2
where the time goes:
time: 253 us; the launch traced here: 250 us
  waiting for transfers between devices  138 us (55%)
  matrix products  36 us (14%)
  blocking collectives  18.3 us (7%)
  other arithmetic  15.2 us (6%)
  local copies, waits for them, and re-layouts  15 us (6%)
  between operations  14 us (6%)
  starting transfers between devices  13.7 us (5%)
    ppermute x6, waiting for transfers between devices, turned(): lax.ppermute(value, axis, [(i, (i + by) % devices) for i in range(devices)])  45.1 us
    reduce_scatter x1, waiting for transfers between devices, local(): pair = lax.psum_scatter(pair, 'tp', scatter_dimension=0, tiled=True)  39.1 us
    all_gather x1, waiting for transfers between devices, local(): others = lax.all_gather(moved, 'tp', axis=0, tiled=True)  28.2 us
    reduce_scatter x1, waiting for transfers between devices, local(): back = lax.psum_scatter(part, 'tp', scatter_dimension=0, tiled=True)  25.8 us
    all_gather x1, blocking collectives, local(): coefs = lax.all_gather(coefs, ('ep', 'tp'), axis=0, tiled=True)  18.3 us
    dot_general x2, matrix products, expert_part(): part = jnp.dot(hidden, down_weight[0], preferred_element_type=jnp.float32)  17.6 us
    ppermute x6, starting transfers between devices, turned(): lax.ppermute(value, axis, [(i, (i + by) % devices) for i in range(devices)])  9.98 us
    dot_general x2, matrix products, expert_hidden(): gate = jnp.dot(rows, w_gate, preferred_element_type=jnp.float32)  7.26 us
  transfers between devices with their start and end apart: 11, of which 7 were waited for; matrix products, arithmetic and copies ran while one was open for 14% of the time, Pallas kernels for 0%

commit v1 on v0

--- a/solution.py
+++ b/solution.py
@@ -1,6 +1,8 @@
 import jax
 import jax.numpy as jnp
 from jax import lax
+from jax.experimental import pallas as pl
+from jax.experimental.pallas import tpu as pltpu
 from jax.sharding import PartitionSpec as P
 
 WINDOW_MAX = 16
@@ -164,6 +166,605 @@
     return (mixed_tokens, expert_mix)
 
 
+MESH = pl.DeviceIdType.MESH
+PIECES_GU = 8
+PIECES_D = 4
+PIECES = PIECES_GU + PIECES_D
+WINDOW = 4
+HALVES = 2
+
+
+def fused_kernel(
+    mixer_tokens,
+    mixer_gain,
+    in_weight,
+    group_weight,
+    channel_scale,
+    out_weight,
+    expert_tokens,
+    expert_gain,
+    route_ids,
+    route_weights,
+    gate_weight,
+    up_weight,
+    down_weight,
+    mixed_out,
+    expert_out,
+    mix_raw,
+    exp_raw,
+    w_in,
+    w_group,
+    w_out,
+    w_gu,
+    w_d,
+    tokens,
+    coefs,
+    scales,
+    hid,
+    acc,
+    rs_in,
+    rs_stage,
+    mix_all,
+    pooled_in,
+    mix_part,
+    mix_pair,
+    mix_stage,
+    mix_far,
+    load_sem,
+    x_send,
+    x_recv,
+    y_send,
+    y_recv,
+    own_send,
+    own_recv,
+    fx_send,
+    fx_recv,
+    fy_send,
+    fy_recv,
+    ag_send,
+    ag_recv,
+    coef_send,
+    coef_recv,
+    rs_send,
+    rs_recv,
+    mix_send,
+    mix_recv,
+):
+    f32, bf16 = jnp.float32, jnp.bfloat16
+    rows, width = exp_raw.shape
+    half_rows = rows // HALVES
+    group_width = w_group.shape[0]
+    ff_half = w_d.shape[1] // 2
+    blocks = tokens.shape[0]
+    g = lax.axis_index("grp")
+    e = lax.axis_index("ep")
+    t = lax.axis_index("tp")
+    x = t // 2
+    c = t % 2
+    t_c = 2 * x + 1 - c
+    t_x = 2 * (1 - x) + c
+    t_d = 2 * (1 - x) + 1 - c
+    dev_c, dev_x, dev_y = (g, e, t_c), (g, e, t_x), (1 - g, e, t)
+    hi = e // 2
+    sign = 1 - 2 * hi
+    last = blocks - 1
+
+    def mirror(m):
+        return hi * last + sign * m
+
+    u = mirror(e)
+    end = u == 0
+    mid = u == 1
+    far = (g, lax.rem(e + sign + blocks, blocks), t)
+    near = (g, lax.rem(e - sign + blocks, blocks), t)
+    third = mirror(1 - u)
+
+    def rc(src, dst, send, recv, dev):
+        return pltpu.make_async_remote_copy(
+            src_ref=src, dst_ref=dst, send_sem=send, recv_sem=recv, device_id=dev, device_id_type=MESH
+        )
+
+    def loads():
+        out = []
+        for h in range(2):
+            hh = g if h == 0 else 1 - g
+            lane = pl.multiple_of(hh * ff_half, ff_half)
+            out.append((gate_weight.at[0, :, pl.ds(lane, ff_half)], w_gu.at[t, hh, :, pl.ds(0, ff_half)]))
+            out.append((up_weight.at[0, :, pl.ds(lane, ff_half)], w_gu.at[t, hh, :, pl.ds(ff_half, ff_half)]))
+        out.append((expert_tokens, exp_raw))
+        out.append((down_weight.at[0], w_d.at[t]))
+        out.append((mixer_tokens, mix_raw))
+        out.append((in_weight, w_in))
+        out.append((group_weight.at[0], w_group))
+        out.append((out_weight, w_out))
+        return [pltpu.make_async_copy(a, b, load_sem.at[i]) for i, (a, b) in enumerate(out)]
+
+    local = loads()
+    for copy in local:
+        copy.start()
+    pooled_in[pl.ds(0, rows), :] = jnp.zeros((rows, group_width), bf16)
+
+    barrier = pltpu.get_barrier_semaphore()
+    greet = [dev_c, dev_x, dev_y] + [(g, lax.rem(e + k, blocks), t) for k in range(1, blocks)]
+    for dev in greet:
+        pl.semaphore_signal(barrier, inc=1, device_id=dev, device_id_type=MESH)
+    pl.semaphore_wait(barrier, len(greet))
+
+    def piece(q, h, s):
+        if s < PIECES_GU:
+            n = width // PIECES_GU
+            return w_gu.at[q, h, pl.ds(s * n, n), :]
+        n = ff_half // PIECES_D
+        start = pl.multiple_of(h * ff_half + (s - PIECES_GU) * n, n)
+        return w_d.at[q, pl.ds(start, n), :]
+
+    def send_x(s):
+        p = piece(t, g, s)
+        return rc(p, p, x_send.at[s], x_recv.at[s], dev_x)
+
+    def got_x(s):
+        p = piece(t_x, g, s)
+        return rc(p, p, x_send.at[s], x_recv.at[s], dev_x)
+
+    def send_y(s):
+        p = piece(t_x, g, s)
+        return rc(p, p, y_send.at[s], y_recv.at[s], dev_y)
+
+    def got_y(s):
+        p = piece(t_x, 1 - g, s)
+        return rc(p, p, y_send.at[s], y_recv.at[s], dev_y)
+
+    def send_fx(s):
+        p = piece(t_x, g, s)
+        return rc(p, p, fx_send.at[s], fx_recv.at[s], dev_c)
+
+    def got_fx(s):
+        p = piece(t_d, g, s)
+        return rc(p, p, fx_send.at[s], fx_recv.at[s], dev_c)
+
+    def send_fy(s):
+        p = piece(t_x, 1 - g, s)
+        return rc(p, p, fy_send.at[s], fy_recv.at[s], dev_c)
+
+    def got_fy(s):
+        p = piece(t_d, 1 - g, s)
+        return rc(p, p, fy_send.at[s], fy_recv.at[s], dev_c)
+
+    def own_gu(q):
+        return rc(w_gu.at[q], w_gu.at[q], own_send.at[0], own_recv.at[0], dev_c)
+
+    def own_d(q):
+        return rc(w_d.at[q], w_d.at[q], own_send.at[1], own_recv.at[1], dev_c)
+
+    def norm(raw, gain, dst, start, count):
+        step = 16
+
+        @pl.loop(0, count // step)
+        def _(i):
+            at = pl.ds(pl.multiple_of(start + i * step, step), step)
+            values = raw[at, :].astype(f32)
+            scaled = values * lax.rsqrt(jnp.mean(values * values, axis=-1, keepdims=True) + 1e-06)
+            dst[at, :] = (scaled * gain[...].astype(f32)).astype(bf16)
+
+    def chunk(home, j):
+        return tokens.at[home, pl.ds(j * half_rows, half_rows), :]
+
+    def ag_far(home, j, f):
+        p = chunk(home, j)
+        return rc(p, p, ag_send.at[f], ag_recv.at[f + 6 * (1 - u)], far)
+
+    def ag_near(home, j, f):
+        p = chunk(home, j)
+        return rc(p, p, ag_send.at[4 + f], ag_recv.at[f], near)
+
+    def ag_got(home, j, f):
+        p = chunk(home, j)
+        return rc(p, p, ag_send.at[0], ag_recv.at[f], far)
+
+    local[0].wait()
+    local[1].wait()
+    for s in range(WINDOW):
+        send_x(s).start()
+    local[4].wait()
+    for j in range(HALVES):
+        norm(exp_raw, expert_gain, tokens.at[e], j * half_rows, half_rows)
+        ag_far(e, j, j).start()
+
+        @pl.when(mid)
+        def _():
+            ag_near(e, j, j).start()
+
+    local[2].wait()
+    local[3].wait()
+    own_gu(t).start()
+    local[5].wait()
+    own_d(t).start()
+
+    ids = route_ids[...]
+    weights = route_weights[...]
+    shares = weights / jnp.sum(weights, axis=1, keepdims=True)
+    lanes = lax.broadcasted_iota(jnp.int32, (rows, rows), 1)
+    coef = jnp.zeros((rows, rows), f32)
+    for k in range(ids.shape[1]):
+        coef = coef + jnp.where(ids[:, k : k + 1] == lanes, shares[:, k : k + 1], 0.0)
+    coefs[e] = jnp.transpose(coef)[: coefs.shape[1], :]
+
+    def coef_to(k):
+        dev = (g, lax.rem(e + k, blocks), t)
+        return rc(coefs.at[e], coefs.at[e], coef_send.at[k - 1], coef_recv.at[k - 1], dev)
+
+    def coef_got(k):
+        home = lax.rem(e - k + blocks, blocks)
+        return rc(coefs.at[home], coefs.at[home], coef_send.at[k - 1], coef_recv.at[k - 1], dev_c)
+
+    for k in range(1, blocks):
+        coef_to(k).start()
+
+    local[6].wait()
+    norm(mix_raw, mixer_gain, mix_all.at[t], 0, rows)
+
+    def mix_x(q, j):
+        p = mix_all.at[q, pl.ds(j * half_rows, half_rows), :]
+        return rc(p, p, mix_send.at[j], mix_recv.at[j], dev_x)
+
+    def mix_fwd(q, j):
+        p = mix_all.at[q, pl.ds(j * half_rows, half_rows), :]
+        return rc(p, p, mix_send.at[2 + j], mix_recv.at[2 + j], dev_c)
+
+    def mix_own(q):
+        return rc(mix_all.at[q], mix_all.at[q], mix_send.at[4], mix_recv.at[4], dev_c)
+
+    mix_own(t).start()
+
+    def hidden(home, xq):
+        @pl.loop(0, 4)
+        def _(j):
+            q = 2 * xq + j // 2
+            h = j % 2
+            both = jnp.dot(tokens[home], w_gu[q, h], preferred_element_type=f32)
+            gate, upper = both[:, :ff_half], both[:, ff_half:]
+            value = gate / (1.0 + jnp.exp(-gate)) * upper
+            hid[home, xq, :, pl.ds(pl.multiple_of(j * ff_half, ff_half), ff_half)] = value.astype(bf16)
+
+    col = 512
+
+    def down(home, xq, first):
+        @pl.loop(0, width // col)
+        def _(n):
+            at = pl.ds(pl.multiple_of(n * col, col), col)
+            w = w_d[pl.ds(2 * xq, 2), :, at].reshape(4 * ff_half, col)
+            part = jnp.dot(hid[home, xq], w, preferred_element_type=f32)
+            if first:
+                acc[home, :, at] = part
+            else:
+                scale = scales[home][:, :1]
+                acc[home, :, at] = (acc[home, :, at] + part) * scale
+
+    def pool_in(xq):
+        @pl.loop(0, 2)
+        def _(j):
+            q = 2 * xq + j
+            value = jnp.dot(mix_all[q], w_in[...], preferred_element_type=f32)
+            pooled_in[pl.ds(pl.multiple_of(rows * (q + 1), rows), rows), :] = value.astype(bf16)
+
+    def wait_fgu():
+        for s in range(PIECES_GU):
+            got_fx(s).wait_recv()
+            got_fy(s).wait_recv()
+
+    for s in range(PIECES):
+        got_x(s).wait_recv()
+        send_y(s).start()
+        send_fx(s).start()
+        if s + WINDOW < PIECES:
+            send_x(s + WINDOW).start()
+        elif s + WINDOW < PIECES + HALVES:
+            mix_x(t, s + WINDOW - PIECES).start()
+        if s >= 1:
+            got_y(s - 1).wait_recv()
+            send_fy(s - 1).start()
+        if s % 2 == 1:
+            f = s // 2
+
+            @pl.when(end)
+            def _():
+                ag_got(mirror(1 + f // 2), f % 2, f).wait_recv()
+
+            if f < 4:
+
+                @pl.when(mid)
+                def _():
+                    home = mirror(2 + f // 2)
+                    ag_got(home, f % 2, f).wait_recv()
+                    ag_near(home, f % 2, f + 2).start()
+
+            if f < 2:
+
+                @pl.when(mid)
+                def _():
+                    home = mirror(0)
+                    ag_got(home, f % 2, 6 + f).wait_recv()
+                    ag_far(home, f % 2, 2 + f).start()
+
+        if s == 1:
+            for k in range(1, blocks):
+                coef_got(k).wait_recv()
+            for home in range(blocks):
+                row = coefs[home, pl.ds(e, 1), :]
+                scales[home] = jnp.transpose(jnp.broadcast_to(row, (rows, rows)))
+        if s == 2:
+            own_gu(t_c).wait_recv()
+            own_d(t_c).wait_recv()
+            hidden(e, x)
+        if s == 3:
+            down(e, x, True)
+        if s == 4:
+            hidden(third, x)
+        if s == 5:
+            down(third, x, True)
+        if s == 6:
+            mix_own(t_c).wait_recv()
+            local[7].wait()
+            pool_in(x)
+        if s == 8:
+            hidden(mirror(2), x)
+            down(mirror(2), x, True)
+        if s == 9:
+            wait_fgu()
+            hidden(mirror(2), 1 - x)
+        if s == 10:
+            hidden(third, 1 - x)
+            hidden(e, 1 - x)
+
+    got_y(PIECES - 1).wait_recv()
+    send_fy(PIECES - 1).start()
+    hidden(mirror(3), x)
+    for s in range(PIECES_GU, PIECES):
+        got_fx(s).wait_recv()
+        got_fy(s).wait_recv()
+
+    def rs_far(k):
+        p = rs_stage.at[k]
+        return rc(p, rs_in.at[k + 6 * u], rs_send.at[k], rs_recv.at[k + 6 * u], far)
+
+    def rs_near(k):
+        p = rs_stage.at[4 + k]
+        return rc(p, rs_in.at[6 + k], rs_send.at[4 + k], rs_recv.at[6 + k], near)
+
+    def rs_got(k):
+        return rc(rs_in.at[k], rs_in.at[k], rs_send.at[0], rs_recv.at[k], far)
+
+    def first_send(home, k):
+        @pl.when(end)
+        def _():
+            for j in range(HALVES):
+                at = pl.ds(j * half_rows, half_rows)
+                rs_stage[k + j] = acc[home, at, :].astype(bf16)
+                rs_far(k + j).start()
+
+    def lead(k):
+        @pl.when(mid)
+        def _():
+            rs_got(k).wait_recv()
+            if k < 4:
+                at = pl.ds((k % 2) * half_rows, half_rows)
+                rs_stage[k] = (acc[mirror(2 + k // 2), at, :] + rs_in[k].astype(f32)).astype(bf16)
+                rs_far(k).start()
+
+    def lag(k):
+        @pl.when(mid)
+        def _():
+            rs_got(6 + k).wait_recv()
+            if k >= 2:
+                at = pl.ds((k % 2) * half_rows, half_rows)
+                rs_stage[4 + k - 2] = (acc[mirror(0), at, :] + rs_in[6 + k].astype(f32)).astype(bf16)
+                rs_near(k - 2).start()
+
+    down(mirror(2), 1 - x, False)
+    first_send(mirror(2), 0)
+    hidden(mirror(3), 1 - x)
+    down(mirror(3), x, True)
+    down(mirror(3), 1 - x, False)
+    first_send(mirror(3), 2)
+    down(third, 1 - x, False)
+    first_send(third, 4)
+    down(e, 1 - x, False)
+
+    for j in range(HALVES):
+        mix_x(t_x, j).wait_recv()
+        mix_fwd(t_x, j).start()
+    lead(0)
+
+    def rim_to():
+        return rc(
+            pooled_in.at[pl.ds(rows * (blocks + 1) - 16, 16), :],
+            pooled_in.at[pl.ds(rows - 16, 16), :],
+            mix_send.at[5],
+            mix_recv.at[5],
+            (g, lax.rem(e + 1, blocks), t),
+        )
+
+    for j in range(HALVES):
+        mix_fwd(t_d, j).wait_recv()
+    pool_in(1 - x)
+
+    @pl.when(e < last)
+    def _():
+        rim_to().start()
+
+    lead(1)
+
+    @pl.when(e > 0)
+    def _():
+        rim_to().wait_recv()
+
+    local[8].wait()
+    local[9].wait()
+    window = 2 + 2 * jnp.minimum(t, 1) + 4 * (t // 2) + 8 * (t // 3)
+
+    def mix_down(j):
+        q = (2 * (1 - x) if j < 2 else 2 * x) + (1 - c if j % 2 == 0 else c)
+        start = pl.multiple_of(q * rows, rows)
+        seg = pooled_in[pl.ds(start, 2 * rows), :]
+        i = lax.broadcasted_iota(jnp.int32, (rows, 2 * rows), 0) + rows
+        k = lax.broadcasted_iota(jnp.int32, (rows, 2 * rows), 1)
+        band = jnp.where((k <= i) & (k > i - window), 1.0, 0.0).astype(bf16)
+        sums = jnp.dot(band, seg, preferred_element_type=f32)
+        place = lax.broadcasted_iota(jnp.int32, (rows, 1), 0) + (e * blocks + q) * rows + 1
+        counts = jnp.minimum(place, window).astype(f32)
+        pooled = (sums / counts - seg[rows:, :].astype(f32)).astype(bf16)
+        grouped = jnp.dot(pooled, w_group[...], preferred_element_type=f32)
+        grouped = (grouped * channel_scale[...].astype(f32)).astype(bf16)
+
+        @pl.loop(0, width // col)
+        def _(n):
+            at = pl.ds(pl.multiple_of(n * col, col), col)
+            mix_part[j, :, at] = jnp.dot(grouped, w_out[:, at], preferred_element_type=f32).astype(bf16)
+
+    def pair_to(j):
+        return rc(mix_part.at[2 * j], mix_pair.at[j], mix_send.at[6 + j], mix_recv.at[6 + j], dev_c)
+
+    def cross(j):
+        at = pl.ds(j * half_rows, half_rows)
+        return rc(mix_stage.at[at, :], mix_far.at[at, :], mix_send.at[8 + j], mix_recv.at[8 + j], dev_x)
+
+    mix_down(0)
+    pair_to(0).start()
+    mix_down(1)
+    pair_to(0).wait_recv()
+    for j in range(HALVES):
+        at = pl.ds(j * half_rows, half_rows)
+        mix_stage[at, :] = (mix_part[1, at, :].astype(f32) + mix_pair[0, at, :].astype(f32)).astype(bf16)
+        cross(j).start()
+    lag(0)
+    lead(2)
+    mix_down(2)
+    pair_to(1).start()
+    mix_down(3)
+    lag(1)
+    lead(3)
+    lag(2)
+    lead(4)
+    lag(3)
+    pair_to(1).wait_recv()
+    for j in range(HALVES):
+        at = pl.ds(j * half_rows, half_rows)
+        cross(j).wait_recv()
+        mixed_out[at, :] = (
+            mix_part[3, at, :].astype(f32) + mix_pair[1, at, :].astype(f32) + mix_far[at, :].astype(f32)
+        ).astype(bf16)
+    lead(5)
+    for j in range(HALVES):
+        at = pl.ds(j * half_rows, half_rows)
+
+        @pl.when(mid)
+        def _():
+            expert_out[at, :] = (acc[e, at, :] + rs_in[4 + j].astype(f32) + rs_in[6 + j].astype(f32)).astype(bf16)
+
+        @pl.when(end)
+        def _():
+            rs_got(6 + j).wait_recv()
+            expert_out[at, :] = (acc[e, at, :] + rs_in[6 + j].astype(f32)).astype(bf16)
+
+    for s in range(PIECES):
+        send_x(s).wait_send()
+        send_y(s).wait_send()
+        send_fx(s).wait_send()
+        send_fy(s).wait_send()
+    own_gu(t).wait_send()
+    own_d(t).wait_send()
+    for k in range(1, blocks):
+        coef_to(k).wait_send()
+    for j in range(HALVES):
+        ag_far(e, j, j).wait_send()
+        mix_x(t, j).wait_send()
+        mix_fwd(t_x, j).wait_send()
+        pair_to(j).wait_send()
+        cross(j).wait_send()
+    mix_own(t).wait_send()
+
+    @pl.when(e < last)
+    def _():
+        rim_to().wait_send()
+
+    @pl.when(end)
+    def _():
+        for k in range(6):
+            rs_far(k).wait_send()
+
+    @pl.when(mid)
+    def _():
+        for f in range(6):
+            ag_near(e, f % 2, f).wait_send()
+        for f in range(2):
+            ag_far(e, f, 2 + f).wait_send()
+        for k in range(4):
+            rs_far(k).wait_send()
+        for k in range(2):
+            rs_near(k).wait_send()
+
+
+def fused(*args):
+    (mixer_tokens, _, in_weight, group_weight, _, out_weight, _, _, route_ids, _, gate_weight, _, _) = args
+    rows, width = mixer_tokens.shape
+    group_width = in_weight.shape[1]
+    ff = gate_weight.shape[2]
+    blocks = lax.axis_size("ep")
+    parts = lax.axis_size("tp")
+    half = rows // HALVES
+    bf16, f32 = jnp.bfloat16, jnp.float32
+    vmem = pltpu.VMEM
+    dma = pltpu.SemaphoreType.DMA
+    anyspace = pl.BlockSpec(memory_space=pl.ANY)
+    local_spec = pl.BlockSpec(memory_space=pltpu.VMEM)
+    args = list(args)
+    for i in (1, 4, 7):
+        args[i] = args[i].reshape(1, -1)
+    small = (1, 4, 7, 8, 9)
+    scratch = [
+        vmem((rows, width), bf16),
+        vmem((rows, width), bf16),
+        vmem((width, group_width), bf16),
+        vmem((group_width, group_width), bf16),
+        vmem((group_width, width), bf16),
+        vmem((parts, 2, width, ff), bf16),
+        vmem((parts, ff, width), bf16),
+        vmem((blocks, rows, width), bf16),
+        vmem((blocks, 8, rows), f32),
+        vmem((blocks, rows, rows), f32),
+        vmem((blocks, 2, rows, 2 * ff), bf16),
+        vmem((blocks, rows, width), f32),
+        vmem((10, half, width), bf16),
+        vmem((6, half, width), bf16),
+        vmem((parts, rows, width), bf16),
+        vmem((rows * (parts + 1), group_width), bf16),
+        vmem((parts, rows, width), bf16),
+        vmem((2, rows, width), bf16),
+        vmem((rows, width), bf16),
+        vmem((rows, width), bf16),
+        dma((10,)),
+    ]
+    for count in (PIECES, PIECES, PIECES, PIECES, 2, 2, PIECES, PIECES, PIECES, PIECES, 10, 8, 3, 3, 6, 10, 10, 10):
+        scratch.append(dma((count,)))
+    shape = jax.ShapeDtypeStruct((rows, width), bf16)
+    return pl.pallas_call(
+        fused_kernel,
+        out_shape=(shape, shape),
+        in_specs=[local_spec if i in small else anyspace for i in range(len(args))],
+        out_specs=(local_spec, local_spec),
+        scratch_shapes=scratch,
+        compiler_params=pltpu.CompilerParams(
+            collective_id=0, has_side_effects=True, vmem_limit_bytes=60 << 20
+        ),
+        name="fused",
+    )(*args)
+
+
+def fits(mesh):
+    sizes = dict(mesh.shape)
+    return sizes["grp"] == 2 and sizes["ep"] == 4 and sizes["tp"] == 4
+
+
 def solution(mesh):
     placed = (
         P(("grp", "ep", "tp"), None),
@@ -181,7 +782,7 @@
         P("ep", "tp", None),
     )
     return jax.shard_map(
-        local,
+        fused if fits(mesh) else local,
         mesh=mesh,
         in_specs=placed,
         out_specs=(P(("grp", "ep", "tp"), None), P(("grp", "ep", "tp"), None)),

time: 253 us -> 127 us (0.50)
  the two profiles are of different devices: /device:TPU:8 before, /device:TPU:26 now
where the time goes in v1:
time: 127 us
  Pallas kernels  116 us (91%)
  local copies, waits for them, and re-layouts  10.4 us (8%)
    pallas_call x1, Pallas kernels, fused(): pl.pallas_call(fused_kernel, out_shape=(shape, shape), in_specs=[local_sp...  116 us
    unnamed x4, local copies, waits for them, and re-layouts  6.59 us
    reshape x3, local copies, waits for them, and re-layouts, fused(): args[i] = args[i].reshape(1, -1)  3.83 us

profile of v1, /device:TPU:26, one launch (start us, length us, event | category | flops | bytes accessed | tf_op | source)
XLA Modules:
  0.0 126.7 jit_solution(9133934355133622259)
XLA Ops:
  0.6 1.3 reshape.14.channel_scale
  1.9 1.3 %reshape.13.mixer_gain = bf16[1,2048]{1,0:T(2,128)(2,1)} reshape(bf16[2048]{0:T(1024)(128)(2,1)} %param.14) | data formatting | bytes 8192 | tf_op jit(solution)/shard_map/reshape | solution.py:722
  3.2 1.3 %reshape.15.expert_gain = bf16[1,2048]{1,0:T(2,128)(2,1)} reshape(bf16[2048]{0:T(1024)(128)(2,1)} %param.20) | data formatting | bytes 8192 | tf_op jit(solution)/shard_map/reshape | solution.py:722
  4.5 1.4 %copy.15.route_ids = s32[128,2]{1,0:T(8,128)} copy(s32[128,2]{0,1:T(2,128)} %param.21) | data formatting | bytes 2048 | tf_op args[8]
  5.9 1.4 %copy.16.route_weights = f32[128,2]{1,0:T(8,128)} copy(f32[128,2]{0,1:T(2,128)} %param.22) | data formatting | bytes 2048 | tf_op args[9]
  7.3 115.6 %fused.1 = (bf16[128,2048]{1,0:T(8,128)(2,1)}, bf16[128,2048]{1,0:T(8,128)(2,1)}) custom-call(bf16[128,2048]{1,0:T(8,128)(2,1)} %mixer_tokens.1, bf16[1,2048]{1,0:T(2,128)(2,1)} %reshape.13.mixer_gain, bf16[2048,512]{1,0:T(8,128)(2,1)} %in_weight.1, bf16[1,512,512]{2,1,0:T(8,128)(2,1)} %group_weight.1, bf16[1,512]{1,0:T(2,128)(2,1)} %reshape.14.channel_scale, ...), custom_call_target="tpu_custom_call" | custom-call | tf_op jit(solution)/shard_map/fused/pallas_call | solution.py:750
  122.9 1.9 %copy.19 = bf16[128,2048]{1,0:T(8,128)(2,1)} copy(bf16[128,2048]{1,0:T(8,128)(2,1)} %get-tuple-element.4) | data formatting | bytes 1048576
  124.8 1.9 %copy.20 = bf16[128,2048]{1,0:T(8,128)(2,1)} copy(bf16[128,2048]{1,0:T(8,128)(2,1)} %get-tuple-element.5) | data formatting | bytes 1048576

commit v2 on v1

--- a/solution.py
+++ b/solution.py
@@ -171,6 +171,7 @@
 PIECES_D = 4
 PIECES = PIECES_GU + PIECES_D
 WINDOW = 4
+LAG = 3
 HALVES = 2
 
 
@@ -210,6 +211,7 @@
     mix_pair,
     mix_stage,
     mix_far,
+    rim_rows,
     load_sem,
     x_send,
     x_recv,
@@ -229,6 +231,8 @@
     rs_recv,
     mix_send,
     mix_recv,
+    rim_send,
+    rim_recv,
 ):
     f32, bf16 = jnp.float32, jnp.bfloat16
     rows, width = exp_raw.shape
@@ -236,6 +240,7 @@
     group_width = w_group.shape[0]
     ff_half = w_d.shape[1] // 2
     blocks = tokens.shape[0]
+    parts = mix_all.shape[0]
     g = lax.axis_index("grp")
     e = lax.axis_index("ep")
     t = lax.axis_index("tp")
@@ -263,6 +268,11 @@
         return pltpu.make_async_remote_copy(
             src_ref=src, dst_ref=dst, send_sem=send, recv_sem=recv, device_id=dev, device_id_type=MESH
         )
+
+    barrier = pltpu.get_barrier_semaphore()
+    greet = [dev_c, dev_x, dev_y] + [(g, lax.rem(e + k, blocks), t) for k in range(1, blocks)]
+    for dev in greet:
+        pl.semaphore_signal(barrier, inc=1, device_id=dev, device_id_type=MESH)
 
     def loads():
         out = []
@@ -282,13 +292,27 @@
     local = loads()
     for copy in local:
         copy.start()
-    pooled_in[pl.ds(0, rows), :] = jnp.zeros((rows, group_width), bf16)
-
-    barrier = pltpu.get_barrier_semaphore()
-    greet = [dev_c, dev_x, dev_y] + [(g, lax.rem(e + k, blocks), t) for k in range(1, blocks)]
-    for dev in greet:
-        pl.semaphore_signal(barrier, inc=1, device_id=dev, device_id_type=MESH)
-    pl.semaphore_wait(barrier, len(greet))
+    def norm(raw, gain, dst, start, count):
+        step = 16
+        gain_row = gain[...].astype(f32).reshape(1, width)
+
+        @pl.loop(0, count // step)
+        def _(i):
+            at = pl.ds(pl.multiple_of(start + i * step, step), step)
+            values = raw[at, :].astype(f32)
+            scaled = values * lax.rsqrt(jnp.mean(values * values, axis=-1, keepdims=True) + 1e-06)
+            dst[at, :] = (scaled * gain_row).astype(bf16)
+
+    local[4].wait()
+    norm(exp_raw, expert_gain, tokens.at[e], 0, rows)
+    ids = route_ids[...]
+    weights = route_weights[...]
+    shares = weights / jnp.sum(weights, axis=0, keepdims=True)
+    numbers = lax.broadcasted_iota(jnp.int32, coefs.shape[1:], 0)
+    coef = jnp.zeros(coefs.shape[1:], f32)
+    for k in range(ids.shape[0]):
+        coef = coef + jnp.where(ids[k : k + 1, :] == numbers, shares[k : k + 1, :], 0.0)
+    coefs[e] = coef
 
     def piece(q, h, s):
         if s < PIECES_GU:
@@ -336,16 +360,6 @@
     def own_d(q):
         return rc(w_d.at[q], w_d.at[q], own_send.at[1], own_recv.at[1], dev_c)
 
-    def norm(raw, gain, dst, start, count):
-        step = 16
-
-        @pl.loop(0, count // step)
-        def _(i):
-            at = pl.ds(pl.multiple_of(start + i * step, step), step)
-            values = raw[at, :].astype(f32)
-            scaled = values * lax.rsqrt(jnp.mean(values * values, axis=-1, keepdims=True) + 1e-06)
-            dst[at, :] = (scaled * gain[...].astype(f32)).astype(bf16)
-
     def chunk(home, j):
         return tokens.at[home, pl.ds(j * half_rows, half_rows), :]
 
@@ -361,13 +375,43 @@
         p = chunk(home, j)
         return rc(p, p, ag_send.at[0], ag_recv.at[f], far)
 
+    rim_source = (t == parts - 1) & (e < last)
+    rim_mine = (t == parts - 1) & (e > 0)
+    rim_relay = (t == parts // 2 - 1) & (e > 0)
+    rim_last = (c == 0) & (e > 0)
+
+    def rim_to(k):
+        src = mix_all.at[t, pl.ds(rows - rim_rows.shape[0], rim_rows.shape[0]), :] if k == 0 else rim_rows
+        dev = ((g, lax.rem(e + 1, blocks), t), dev_x, dev_c)[k]
+        return rc(src, rim_rows, rim_send.at[k], rim_recv.at[k], dev)
+
+    def coef_to(k):
+        dev = (g, lax.rem(e + k, blocks), t)
+        return rc(coefs.at[e], coefs.at[e], coef_send.at[k - 1], coef_recv.at[k - 1], dev)
+
+    def coef_got(k):
+        home = lax.rem(e - k + blocks, blocks)
+        return rc(coefs.at[home], coefs.at[home], coef_send.at[k - 1], coef_recv.at[k - 1], dev_c)
+
+    def mix_x(q, j):
+        p = mix_all.at[q, pl.ds(j * half_rows, half_rows), :]
+        return rc(p, p, mix_send.at[j], mix_recv.at[j], dev_x)
+
+    def mix_fwd(q, j):
+        p = mix_all.at[q, pl.ds(j * half_rows, half_rows), :]
+        return rc(p, p, mix_send.at[2 + j], mix_recv.at[2 + j], dev_c)
+
+    def mix_own(q):
+        return rc(mix_all.at[q], mix_all.at[q], mix_send.at[4], mix_recv.at[4], dev_c)
+
     local[0].wait()
     local[1].wait()
+    pl.semaphore_wait(barrier, len(greet))
     for s in range(WINDOW):
         send_x(s).start()
-    local[4].wait()
+    for k in range(1, blocks):
+        coef_to(k).start()
     for j in range(HALVES):
-        norm(exp_raw, expert_gain, tokens.at[e], j * half_rows, half_rows)
         ag_far(e, j, j).start()
 
         @pl.when(mid)
@@ -379,40 +423,12 @@
     own_gu(t).start()
     local[5].wait()
     own_d(t).start()
-
-    ids = route_ids[...]
-    weights = route_weights[...]
-    shares = weights / jnp.sum(weights, axis=1, keepdims=True)
-    lanes = lax.broadcasted_iota(jnp.int32, (rows, rows), 1)
-    coef = jnp.zeros((rows, rows), f32)
-    for k in range(ids.shape[1]):
-        coef = coef + jnp.where(ids[:, k : k + 1] == lanes, shares[:, k : k + 1], 0.0)
-    coefs[e] = jnp.transpose(coef)[: coefs.shape[1], :]
-
-    def coef_to(k):
-        dev = (g, lax.rem(e + k, blocks), t)
-        return rc(coefs.at[e], coefs.at[e], coef_send.at[k - 1], coef_recv.at[k - 1], dev)
-
-    def coef_got(k):
-        home = lax.rem(e - k + blocks, blocks)
-        return rc(coefs.at[home], coefs.at[home], coef_send.at[k - 1], coef_recv.at[k - 1], dev_c)
-
-    for k in range(1, blocks):
-        coef_to(k).start()
-
     local[6].wait()
     norm(mix_raw, mixer_gain, mix_all.at[t], 0, rows)
 
-    def mix_x(q, j):
-        p = mix_all.at[q, pl.ds(j * half_rows, half_rows), :]
-        return rc(p, p, mix_send.at[j], mix_recv.at[j], dev_x)
-
-    def mix_fwd(q, j):
-        p = mix_all.at[q, pl.ds(j * half_rows, half_rows), :]
-        return rc(p, p, mix_send.at[2 + j], mix_recv.at[2 + j], dev_c)
-
-    def mix_own(q):
-        return rc(mix_all.at[q], mix_all.at[q], mix_send.at[4], mix_recv.at[4], dev_c)
+    @pl.when(rim_source)
+    def _():
+        rim_to(0).start()
 
     mix_own(t).start()
 
@@ -452,6 +468,31 @@
             got_fx(s).wait_recv()
             got_fy(s).wait_recv()
 
+    def relay_y(s):
+        got_y(s).wait_recv()
+        send_fy(s).start()
+
+    def gather(f):
+        @pl.when(end)
+        def _():
+            ag_got(mirror(1 + f // 2), f % 2, f).wait_recv()
+
+        if f < 4:
+
+            @pl.when(mid)
+            def _():
+                home = mirror(2 + f // 2)
+                ag_got(home, f % 2, f).wait_recv()
+                ag_near(home, f % 2, f + 2).start()
+
+        if f < 2:
+
+            @pl.when(mid)
+            def _():
+                home = mirror(0)
+                ag_got(home, f % 2, 6 + f).wait_recv()
+                ag_far(home, f % 2, 2 + f).start()
+
     for s in range(PIECES):
         got_x(s).wait_recv()
         send_y(s).start()
@@ -460,32 +501,10 @@
             send_x(s + WINDOW).start()
         elif s + WINDOW < PIECES + HALVES:
             mix_x(t, s + WINDOW - PIECES).start()
-        if s >= 1:
-            got_y(s - 1).wait_recv()
-            send_fy(s - 1).start()
-        if s % 2 == 1:
-            f = s // 2
-
-            @pl.when(end)
-            def _():
-                ag_got(mirror(1 + f // 2), f % 2, f).wait_recv()
-
-            if f < 4:
-
-                @pl.when(mid)
-                def _():
-                    home = mirror(2 + f // 2)
-                    ag_got(home, f % 2, f).wait_recv()
-                    ag_near(home, f % 2, f + 2).start()
-
-            if f < 2:
-
-                @pl.when(mid)
-                def _():
-                    home = mirror(0)
-                    ag_got(home, f % 2, 6 + f).wait_recv()
-                    ag_far(home, f % 2, 2 + f).start()
-
+        if s >= LAG:
+            relay_y(s - LAG)
+        if s >= 2 and s % 2 == 0:
+            gather(s // 2 - 1)
         if s == 1:
             for k in range(1, blocks):
                 coef_got(k).wait_recv()
@@ -494,31 +513,52 @@
                 scales[home] = jnp.transpose(jnp.broadcast_to(row, (rows, rows)))
         if s == 2:
             own_gu(t_c).wait_recv()
+            hidden(e, x)
+        if s == 5:
+
+            @pl.when(rim_mine)
+            def _():
+                rim_to(0).wait_recv()
+                rim_to(1).start()
+                rim_to(2).start()
+
+        if s == 3:
             own_d(t_c).wait_recv()
-            hidden(e, x)
-        if s == 3:
             down(e, x, True)
         if s == 4:
+            pooled_in[pl.ds(0, rows), :] = jnp.zeros((rows, group_width), bf16)
+        if s == 5:
             hidden(third, x)
-        if s == 5:
+        if s == 6:
             down(third, x, True)
-        if s == 6:
+        if s == 7:
             mix_own(t_c).wait_recv()
             local[7].wait()
             pool_in(x)
-        if s == 8:
+        if s == 11:
+
+            @pl.when(rim_relay)
+            def _():
+                rim_to(1).wait_recv()
+                rim_to(2).start()
+
+        if s == 9:
             hidden(mirror(2), x)
             down(mirror(2), x, True)
-        if s == 9:
+        if s == 10:
             wait_fgu()
             hidden(mirror(2), 1 - x)
-        if s == 10:
+        if s == 11:
             hidden(third, 1 - x)
-            hidden(e, 1 - x)
-
-    got_y(PIECES - 1).wait_recv()
-    send_fy(PIECES - 1).start()
+
+    for s in range(PIECES - LAG, PIECES - 1):
+        relay_y(s)
+    hidden(e, 1 - x)
+    gather(5)
     hidden(mirror(3), x)
+    down(mirror(3), x, True)
+    hidden(mirror(3), 1 - x)
+    relay_y(PIECES - 1)
     for s in range(PIECES_GU, PIECES):
         got_fx(s).wait_recv()
         got_fy(s).wait_recv()
@@ -548,24 +588,22 @@
             rs_got(k).wait_recv()
             if k < 4:
                 at = pl.ds((k % 2) * half_rows, half_rows)
-                rs_stage[k] = (acc[mirror(2 + k // 2), at, :] + rs_in[k].astype(f32)).astype(bf16)
+                rs_stage[k] = (acc[mirror(3 - k // 2), at, :] + rs_in[k].astype(f32)).astype(bf16)
                 rs_far(k).start()
 
     def lag(k):
         @pl.when(mid)
         def _():
             rs_got(6 + k).wait_recv()
-            if k >= 2:
+            if k < 2:
                 at = pl.ds((k % 2) * half_rows, half_rows)
-                rs_stage[4 + k - 2] = (acc[mirror(0), at, :] + rs_in[6 + k].astype(f32)).astype(bf16)
-                rs_near(k - 2).start()
-
+                rs_stage[4 + k] = (acc[mirror(0), at, :] + rs_in[6 + k].astype(f32)).astype(bf16)
+                rs_near(k).start()
+
+    down(mirror(3), 1 - x, False)
+    first_send(mirror(3), 0)
     down(mirror(2), 1 - x, False)
-    first_send(mirror(2), 0)
-    hidden(mirror(3), 1 - x)
-    down(mirror(3), x, True)
-    down(mirror(3), 1 - x, False)
-    first_send(mirror(3), 2)
+    first_send(mirror(2), 2)
     down(third, 1 - x, False)
     first_send(third, 4)
     down(e, 1 - x, False)
@@ -575,29 +613,20 @@
         mix_fwd(t_x, j).start()
     lead(0)
 
-    def rim_to():
-        return rc(
-            pooled_in.at[pl.ds(rows * (blocks + 1) - 16, 16), :],
-            pooled_in.at[pl.ds(rows - 16, 16), :],
-            mix_send.at[5],
-            mix_recv.at[5],
-            (g, lax.rem(e + 1, blocks), t),
-        )
-
     for j in range(HALVES):
         mix_fwd(t_d, j).wait_recv()
     pool_in(1 - x)
 
-    @pl.when(e < last)
+    @pl.when(rim_last)
     def _():
-        rim_to().start()
-
-    lead(1)
+        rim_to(2).wait_recv()
 
     @pl.when(e > 0)
     def _():
-        rim_to().wait_recv()
-
+        value = jnp.dot(rim_rows[...], w_in[...], preferred_element_type=f32)
+        pooled_in[pl.ds(rows - rim_rows.shape[0], rim_rows.shape[0]), :] = value.astype(bf16)
+
+    lead(1)
     local[8].wait()
     local[9].wait()
     window = 2 + 2 * jnp.minimum(t, 1) + 4 * (t // 2) + 8 * (t // 3)
@@ -614,7 +643,7 @@
         counts = jnp.minimum(place, window).astype(f32)
         pooled = (sums / counts - seg[rows:, :].astype(f32)).astype(bf16)
         grouped = jnp.dot(pooled, w_group[...], preferred_element_type=f32)
-        grouped = (grouped * channel_scale[...].astype(f32)).astype(bf16)
+        grouped = (grouped * channel_scale[...].astype(f32).reshape(1, group_width)).astype(bf16)
 
         @pl.loop(0, width // col)
         def _(n):
@@ -659,7 +688,7 @@
 
         @pl.when(mid)
         def _():
-            expert_out[at, :] = (acc[e, at, :] + rs_in[4 + j].astype(f32) + rs_in[6 + j].astype(f32)).astype(bf16)
+            expert_out[at, :] = (acc[e, at, :] + rs_in[4 + j].astype(f32) + rs_in[8 + j].astype(f32)).astype(bf16)
 
         @pl.when(end)
         def _():
@@ -683,9 +712,18 @@
         cross(j).wait_send()
     mix_own(t).wait_send()
 
-    @pl.when(e < last)
+    @pl.when(rim_source)
     def _():
-        rim_to().wait_send()
+        rim_to(0).wait_send()
+
+    @pl.when(rim_mine)
+    def _():
+        rim_to(1).wait_send()
+        rim_to(2).wait_send()
+
+    @pl.when(rim_relay)
+    def _():
+        rim_to(2).wait_send()
 
     @pl.when(end)
     def _():
@@ -718,8 +756,8 @@
     anyspace = pl.BlockSpec(memory_space=pl.ANY)
     local_spec = pl.BlockSpec(memory_space=pltpu.VMEM)
     args = list(args)
-    for i in (1, 4, 7):
-        args[i] = args[i].reshape(1, -1)
+    for i in (8, 9):
+        args[i] = args[i].T
     small = (1, 4, 7, 8, 9)
     scratch = [
         vmem((rows, width), bf16),
@@ -742,11 +780,12 @@
         vmem((2, rows, width), bf16),
         vmem((rows, width), bf16),
         vmem((rows, width), bf16),
+        vmem((WINDOW_MAX, width), bf16),
         dma((10,)),
     ]
-    for count in (PIECES, PIECES, PIECES, PIECES, 2, 2, PIECES, PIECES, PIECES, PIECES, 10, 8, 3, 3, 6, 10, 10, 10):
+    for count in (PIECES, PIECES, PIECES, PIECES, 2, 2, PIECES, PIECES, PIECES, PIECES, 10, 8, 3, 3, 6, 10, 10, 10, 3, 3):
         scratch.append(dma((count,)))
-    shape = jax.ShapeDtypeStruct((rows, width), bf16)
+    shape = vmem((rows, width), bf16)
     return pl.pallas_call(
         fused_kernel,
         out_shape=(shape, shape),

time: 127 us -> 89.5 us (0.70)
  the two profiles are of different devices: /device:TPU:26 before, /device:TPU:8 now
where the time goes in v2:
time: 89.5 us; the launch traced here: 89.1 us
  Pallas kernels  86.9 us (97%)
  local copies, waits for them, and re-layouts  1.59 us (2%)
    pallas_call x1, Pallas kernels, fused(): pl.pallas_call(fused_kernel, out_shape=(shape, shape), in_specs=[local_sp...  86.9 us

profile of v2, /device:TPU:8, one launch (start us, length us, event | category | flops | bytes accessed | tf_op | source)
XLA Modules:
  0.0 89.1 jit_solution(6056841981445410855)
XLA Ops:
  0.6 86.9 %fused.1 = (bf16[128,2048]{1,0:T(8,128)(2,1)S(1)}, bf16[128,2048]{1,0:T(8,128)(2,1)S(1)}) custom-call(bf16[128,2048]{1,0:T(8,128)(2,1)} %mixer_tokens.1, bf16[2048]{0:T(1024)(128)(2,1)} %mixer_gain.1, bf16[2048,512]{1,0:T(8,128)(2,1)} %in_weight.1, bf16[1,512,512]{2,1,0:T(8,128)(2,1)} %group_weight.1, bf16[512]{0:T(512)(128)(2,1)} %channel_scale.1, ...), custom_call_target="tpu_custom_call" | custom-call | tf_op jit(solution)/shard_map/fused/pallas_call | solution.py:789
  87.5 0.8 copy.17
  88.3 0.8 copy.18

commit v3 on v2

--- a/solution.py
+++ b/solution.py
@@ -167,12 +167,15 @@
 
 
 MESH = pl.DeviceIdType.MESH
-PIECES_GU = 8
-PIECES_D = 4
-PIECES = PIECES_GU + PIECES_D
-WINDOW = 4
+GU_CUTS = (0, 1, 2, 4, 6, 8, 10, 12, 14, 16)
+PIECES_GU = len(GU_CUTS) - 1
+D_CUTS = (0, 2, 4, 6, 7, 8)
+PIECES = PIECES_GU + len(D_CUTS) - 1
+WINDOW = 5
 LAG = 3
 HALVES = 2
+CUTS = ((0, 1, 2, 4, 6, 8), (0, 2, 4, 6, 7, 8))
+CHUNKS = len(CUTS[0]) - 1
 
 
 def fused_kernel(
@@ -212,6 +215,8 @@
     mix_stage,
     mix_far,
     rim_rows,
+    w_d2,
+    hid_far,
     load_sem,
     x_send,
     x_recv,
@@ -233,6 +238,8 @@
     mix_recv,
     rim_send,
     rim_recv,
+    d2_send,
+    d2_recv,
 ):
     f32, bf16 = jnp.float32, jnp.bfloat16
     rows, width = exp_raw.shape
@@ -314,13 +321,18 @@
         coef = coef + jnp.where(ids[k : k + 1, :] == numbers, shares[k : k + 1, :], 0.0)
     coefs[e] = coef
 
+    def d_cut(s):
+        unit = ff_half // D_CUTS[-1]
+        low, high = D_CUTS[s - PIECES_GU], D_CUTS[s - PIECES_GU + 1]
+        return low * unit, (high - low) * unit
+
     def piece(q, h, s):
         if s < PIECES_GU:
-            n = width // PIECES_GU
-            return w_gu.at[q, h, pl.ds(s * n, n), :]
-        n = ff_half // PIECES_D
-        start = pl.multiple_of(h * ff_half + (s - PIECES_GU) * n, n)
-        return w_d.at[q, pl.ds(start, n), :]
+            unit = width // GU_CUTS[-1]
+            low, high = GU_CUTS[s], GU_CUTS[s + 1]
+            return w_gu.at[q, h, pl.ds(low * unit, (high - low) * unit), :]
+        start, n = d_cut(s)
+        return w_d.at[q, pl.ds(pl.multiple_of(h * ff_half + start, 16), n), :]
 
     def send_x(s):
         p = piece(t, g, s)
@@ -392,6 +404,32 @@
     def coef_got(k):
         home = lax.rem(e - k + blocks, blocks)
         return rc(coefs.at[home], coefs.at[home], coef_send.at[k - 1], coef_recv.at[k - 1], dev_c)
+
+    def d2_half(ref, q, h):
+        return ref.at[q, pl.ds(pl.multiple_of(h * ff_half, ff_half), ff_half), :]
+
+    def d2_piece(ref, s):
+        start, n = d_cut(s)
+        return ref.at[t_x, pl.ds(pl.multiple_of(g * ff_half + start, 16), n), :]
+
+    def d2_own():
+        return rc(d2_half(w_d, t, g), d2_half(w_d2, t, g), d2_send.at[0], d2_recv.at[0], far)
+
+    def d2_relay(s):
+        k = 1 + s - PIECES_GU
+        return rc(d2_piece(w_d, s), d2_piece(w_d2, s), d2_send.at[k], d2_recv.at[k], far)
+
+    def d2_hid(xq, k):
+        return rc(hid.at[third, xq], hid_far.at[xq], d2_send.at[6 + k], d2_recv.at[6 + k], far)
+
+    def d2_y(k, mine):
+        p = d2_half(w_d2, t if k == 0 else t_x, g if mine else 1 - g)
+        return rc(p, p, d2_send.at[8 + k], d2_recv.at[8 + k], dev_y)
+
+    def d2_c(k, mine):
+        q = (t if k % 2 == 0 else t_x) if mine else (t_c if k % 2 == 0 else t_d)
+        p = d2_half(w_d2, q, g if k < 2 else 1 - g)
+        return rc(p, p, d2_send.at[10 + k], d2_recv.at[10 + k], dev_c)
 
     def mix_x(q, j):
         p = mix_all.at[q, pl.ds(j * half_rows, half_rows), :]
@@ -423,6 +461,11 @@
     own_gu(t).start()
     local[5].wait()
     own_d(t).start()
+
+    @pl.when(end)
+    def _():
+        d2_own().start()
+
     local[6].wait()
     norm(mix_raw, mixer_gain, mix_all.at[t], 0, rows)
 
@@ -497,136 +540,139 @@
         got_x(s).wait_recv()
         send_y(s).start()
         send_fx(s).start()
+        if s >= PIECES_GU:
+
+            @pl.when(end)
+            def _():
+                d2_relay(s).start()
+
+        if s + WINDOW == PIECES:
+
+            @pl.when(rim_mine)
+            def _():
+                rim_to(1).start()
+
         if s + WINDOW < PIECES:
             send_x(s + WINDOW).start()
         elif s + WINDOW < PIECES + HALVES:
             mix_x(t, s + WINDOW - PIECES).start()
         if s >= LAG:
             relay_y(s - LAG)
-        if s >= 2 and s % 2 == 0:
+        if s in (3, 5, 7, 9, 11):
             gather(s // 2 - 1)
-        if s == 1:
+        if s == 2:
             for k in range(1, blocks):
                 coef_got(k).wait_recv()
             for home in range(blocks):
                 row = coefs[home, pl.ds(e, 1), :]
                 scales[home] = jnp.transpose(jnp.broadcast_to(row, (rows, rows)))
-        if s == 2:
+        if s == 3:
             own_gu(t_c).wait_recv()
             hidden(e, x)
-        if s == 5:
+        if s == 6:
 
             @pl.when(rim_mine)
             def _():
                 rim_to(0).wait_recv()
-                rim_to(1).start()
                 rim_to(2).start()
 
-        if s == 3:
+        if s == 4:
             own_d(t_c).wait_recv()
             down(e, x, True)
-        if s == 4:
+        if s == 5:
             pooled_in[pl.ds(0, rows), :] = jnp.zeros((rows, group_width), bf16)
-        if s == 5:
+        if s == 6:
             hidden(third, x)
-        if s == 6:
-            down(third, x, True)
+
+            @pl.when(end)
+            def _():
+                d2_hid(x, 0).start()
+
         if s == 7:
+
+            @pl.when(mid)
+            def _():
+                down(third, x, True)
+
+        if s == 8:
             mix_own(t_c).wait_recv()
             local[7].wait()
             pool_in(x)
-        if s == 11:
-
-            @pl.when(rim_relay)
-            def _():
-                rim_to(1).wait_recv()
-                rim_to(2).start()
-
-        if s == 9:
+        if s == 10:
             hidden(mirror(2), x)
             down(mirror(2), x, True)
-        if s == 10:
+        if s == 11:
             wait_fgu()
-            hidden(mirror(2), 1 - x)
-        if s == 11:
             hidden(third, 1 - x)
 
-    for s in range(PIECES - LAG, PIECES - 1):
-        relay_y(s)
-    hidden(e, 1 - x)
+            @pl.when(end)
+            def _():
+                d2_hid(1 - x, 1).start()
+
     gather(5)
     hidden(mirror(3), x)
+    relay_y(PIECES - 3)
     down(mirror(3), x, True)
+    relay_y(PIECES - 2)
     hidden(mirror(3), 1 - x)
     relay_y(PIECES - 1)
+
+    @pl.when(mid)
+    def _():
+        d2_own().wait_recv()
+        d2_y(0, True).start()
+        d2_c(0, True).start()
+
     for s in range(PIECES_GU, PIECES):
         got_fx(s).wait_recv()
         got_fy(s).wait_recv()
 
+    def cut(k):
+        slot, j = divmod(k, CHUNKS)
+        unit = rows // CUTS[slot][-1]
+        low, high = CUTS[slot][j], CUTS[slot][j + 1]
+        return slot, pl.ds(low * unit, (high - low) * unit)
+
     def rs_far(k):
-        p = rs_stage.at[k]
-        return rc(p, rs_in.at[k + 6 * u], rs_send.at[k], rs_recv.at[k + 6 * u], far)
+        slot, at = cut(k)
+        sem = k + 2 * CHUNKS * u
+        return rc(rs_stage.at[slot, at, :], rs_in.at[slot + 2 * u, at, :], rs_send.at[k], rs_recv.at[sem], far)
 
     def rs_near(k):
-        p = rs_stage.at[4 + k]
-        return rc(p, rs_in.at[6 + k], rs_send.at[4 + k], rs_recv.at[6 + k], near)
-
-    def rs_got(k):
-        return rc(rs_in.at[k], rs_in.at[k], rs_send.at[0], rs_recv.at[k], far)
-
-    def first_send(home, k):
+        slot, at = cut(k)
+        sem = 2 * CHUNKS + k
+        return rc(rs_stage.at[2, at, :], rs_in.at[2, at, :], rs_send.at[sem], rs_recv.at[sem], near)
+
+    def rs_got(k, base):
+        slot, at = cut(k)
+        p = rs_in.at[slot + base, at, :]
+        return rc(p, p, rs_send.at[0], rs_recv.at[k + base * CHUNKS], far)
+
+    def first_send(home, first):
         @pl.when(end)
         def _():
-            for j in range(HALVES):
-                at = pl.ds(j * half_rows, half_rows)
-                rs_stage[k + j] = acc[home, at, :].astype(bf16)
-                rs_far(k + j).start()
+            for k in range(first, first + CHUNKS):
+                slot, at = cut(k)
+                rs_stage[slot, at, :] = acc[home, at, :].astype(bf16)
+                rs_far(k).start()
 
     def lead(k):
         @pl.when(mid)
         def _():
-            rs_got(k).wait_recv()
-            if k < 4:
-                at = pl.ds((k % 2) * half_rows, half_rows)
-                rs_stage[k] = (acc[mirror(3 - k // 2), at, :] + rs_in[k].astype(f32)).astype(bf16)
-                rs_far(k).start()
+            rs_got(k, 0).wait_recv()
+            slot, at = cut(k)
+            rs_stage[slot, at, :] = (acc[mirror(3 - slot), at, :] + rs_in[slot, at, :].astype(f32)).astype(bf16)
+            rs_far(k).start()
 
     def lag(k):
         @pl.when(mid)
         def _():
-            rs_got(6 + k).wait_recv()
-            if k < 2:
-                at = pl.ds((k % 2) * half_rows, half_rows)
-                rs_stage[4 + k] = (acc[mirror(0), at, :] + rs_in[6 + k].astype(f32)).astype(bf16)
+            rs_got(k, 2).wait_recv()
+            if k < CHUNKS:
+                slot, at = cut(k)
+                rs_stage[2, at, :] = (acc[mirror(0), at, :] + rs_in[2, at, :].astype(f32)).astype(bf16)
                 rs_near(k).start()
 
-    down(mirror(3), 1 - x, False)
-    first_send(mirror(3), 0)
-    down(mirror(2), 1 - x, False)
-    first_send(mirror(2), 2)
-    down(third, 1 - x, False)
-    first_send(third, 4)
-    down(e, 1 - x, False)
-
-    for j in range(HALVES):
-        mix_x(t_x, j).wait_recv()
-        mix_fwd(t_x, j).start()
-    lead(0)
-
-    for j in range(HALVES):
-        mix_fwd(t_d, j).wait_recv()
-    pool_in(1 - x)
-
-    @pl.when(rim_last)
-    def _():
-        rim_to(2).wait_recv()
-
-    @pl.when(e > 0)
-    def _():
-        value = jnp.dot(rim_rows[...], w_in[...], preferred_element_type=f32)
-        pooled_in[pl.ds(rows - rim_rows.shape[0], rim_rows.shape[0]), :] = value.astype(bf16)
-
-    lead(1)
     local[8].wait()
     local[9].wait()
     window = 2 + 2 * jnp.minimum(t, 1) + 4 * (t // 2) + 8 * (t // 3)
@@ -657,8 +703,62 @@
         at = pl.ds(j * half_rows, half_rows)
         return rc(mix_stage.at[at, :], mix_far.at[at, :], mix_send.at[8 + j], mix_recv.at[8 + j], dev_x)
 
+    def mix_relay(j):
+        mix_x(t_x, j).wait_recv()
+        mix_fwd(t_x, j).start()
+
+    def final(k):
+        @pl.when(mid)
+        def _():
+            _, at = cut(CHUNKS + k)
+            expert_out[at, :] = (acc[e, at, :] + rs_in[3, at, :].astype(f32)).astype(bf16)
+
+        @pl.when(end)
+        def _():
+            _, at = cut(k)
+            rs_got(k, 2).wait_recv()
+            expert_out[at, :] = (acc[e, at, :] + rs_in[2, at, :].astype(f32)).astype(bf16)
+
+    down(mirror(3), 1 - x, False)
+    first_send(mirror(3), 0)
+    hidden(mirror(2), 1 - x)
+    lead(0)
+    down(mirror(2), 1 - x, False)
+    first_send(mirror(2), CHUNKS)
+    mix_relay(0)
+    lead(1)
+
+    @pl.when(mid)
+    def _():
+        down(third, 1 - x, False)
+        for s in range(PIECES_GU, PIECES):
+            d2_relay(s).wait_recv()
+        d2_y(1, True).start()
+        d2_c(1, True).start()
+
+    @pl.when(rim_relay)
+    def _():
+        rim_to(1).wait_recv()
+        rim_to(2).start()
+
+    mix_relay(1)
+    lead(2)
+    for j in range(HALVES):
+        mix_fwd(t_d, j).wait_recv()
+    pool_in(1 - x)
+
+    @pl.when(rim_last)
+    def _():
+        rim_to(2).wait_recv()
+
+    @pl.when(e > 0)
+    def _():
+        value = jnp.dot(rim_rows[...], w_in[...], preferred_element_type=f32)
+        pooled_in[pl.ds(rows - rim_rows.shape[0], rim_rows.shape[0]), :] = value.astype(bf16)
+
     mix_down(0)
     pair_to(0).start()
+    lead(3)
     mix_down(1)
     pair_to(0).wait_recv()
     for j in range(HALVES):
@@ -666,15 +766,58 @@
         mix_stage[at, :] = (mix_part[1, at, :].astype(f32) + mix_pair[0, at, :].astype(f32)).astype(bf16)
         cross(j).start()
     lag(0)
-    lead(2)
+    lag(1)
+    lag(2)
+    lead(4)
+
+    @pl.when(mid)
+    def _():
+        d2_y(0, False).wait_recv()
+        d2_c(2, True).start()
+
+    lag(3)
+    hidden(e, 1 - x)
+    lead(5)
+    down(e, 1 - x, False)
+    lag(4)
     mix_down(2)
     pair_to(1).start()
+    lead(6)
+    lag(5)
     mix_down(3)
-    lag(1)
-    lead(3)
-    lag(2)
-    lead(4)
-    lag(3)
+    lead(7)
+    lag(6)
+
+    @pl.when(mid)
+    def _():
+        d2_y(1, False).wait_recv()
+        d2_c(3, True).start()
+
+    lead(8)
+    lead(9)
+
+    @pl.when(mid)
+    def _():
+        scales[0] = jnp.transpose(jnp.broadcast_to(coefs[e, pl.ds(mirror(0), 1), :], (rows, rows)))
+        d2_hid(x, 0).wait_recv()
+        d2_hid(1 - x, 1).wait_recv()
+        for k in range(4):
+            d2_c(k, False).wait_recv()
+
+        @pl.loop(0, width // col)
+        def _(n):
+            at = pl.ds(pl.multiple_of(n * col, col), col)
+            part = acc[e, :, at]
+            scale = scales[0][:, :1]
+            for xq in range(2):
+                w = w_d2[pl.ds(2 * xq, 2), :, at].reshape(4 * ff_half, col)
+                part = part + jnp.dot(hid_far[xq], w, preferred_element_type=f32) * scale
+            acc[e, :, at] = part
+
+    final(0)
+    final(1)
+    lag(7)
+    final(2)
     pair_to(1).wait_recv()
     for j in range(HALVES):
         at = pl.ds(j * half_rows, half_rows)
@@ -682,19 +825,6 @@
         mixed_out[at, :] = (
             mix_part[3, at, :].astype(f32) + mix_pair[1, at, :].astype(f32) + mix_far[at, :].astype(f32)
         ).astype(bf16)
-    lead(5)
-    for j in range(HALVES):
-        at = pl.ds(j * half_rows, half_rows)
-
-        @pl.when(mid)
-        def _():
-            expert_out[at, :] = (acc[e, at, :] + rs_in[4 + j].astype(f32) + rs_in[8 + j].astype(f32)).astype(bf16)
-
-        @pl.when(end)
-        def _():
-            rs_got(6 + j).wait_recv()
-            expert_out[at, :] = (acc[e, at, :] + rs_in[6 + j].astype(f32)).astype(bf16)
-
     for s in range(PIECES):
         send_x(s).wait_send()
         send_y(s).wait_send()
@@ -727,8 +857,11 @@
 
     @pl.when(end)
     def _():
-        for k in range(6):
-            rs_far(k).wait_send()
+        d2_own().wait_send()
+        d2_hid(x, 0).wait_send()
+        d2_hid(1 - x, 1).wait_send()
+        for s in range(PIECES_GU, PIECES):
+            d2_relay(s).wait_send()
 
     @pl.when(mid)
     def _():
@@ -736,9 +869,21 @@
             ag_near(e, f % 2, f).wait_send()
         for f in range(2):
             ag_far(e, f, 2 + f).wait_send()
+        for k in range(2):
+            d2_y(k, True).wait_send()
         for k in range(4):
-            rs_far(k).wait_send()
-        for k in range(2):
+            d2_c(k, True).wait_send()
+
+    lag(8)
+    final(3)
+    lag(9)
+    final(4)
+    for k in range(2 * CHUNKS):
+        rs_far(k).wait_send()
+
+    @pl.when(mid)
+    def _():
+        for k in range(CHUNKS):
             rs_near(k).wait_send()
 
 
@@ -772,8 +917,8 @@
         vmem((blocks, rows, rows), f32),
         vmem((blocks, 2, rows, 2 * ff), bf16),
         vmem((blocks, rows, width), f32),
-        vmem((10, half, width), bf16),
-        vmem((6, half, width), bf16),
+        vmem((4, rows, width), bf16),
+        vmem((3, rows, width), bf16),
         vmem((parts, rows, width), bf16),
         vmem((rows * (parts + 1), group_width), bf16),
         vmem((parts, rows, width), bf16),
@@ -781,9 +926,11 @@
         vmem((rows, width), bf16),
         vmem((rows, width), bf16),
         vmem((WINDOW_MAX, width), bf16),
+        vmem((parts, ff, width), bf16),
+        vmem((2, rows, 2 * ff), bf16),
         dma((10,)),
     ]
-    for count in (PIECES, PIECES, PIECES, PIECES, 2, 2, PIECES, PIECES, PIECES, PIECES, 10, 8, 3, 3, 6, 10, 10, 10, 3, 3):
+    for count in (PIECES, PIECES, PIECES, PIECES, 2, 2, PIECES, PIECES, PIECES, PIECES, 10, 8, 3, 3, 3 * CHUNKS, 4 * CHUNKS, 10, 10, 3, 3, 14, 14):
         scratch.append(dma((count,)))
     shape = vmem((rows, width), bf16)
     return pl.pallas_call(

time: 89.5 us -> 82.2 us (0.918)
  Pallas kernels: 86.9 us -> 79.8 us
    pallas_call x1, Pallas kernels: 86.9 us -> 79.8 us  [fused(): pl.pallas_call(fused_kernel, out_shape=(shape, shape), in_specs=[local_sp...]
where the time goes in v3:
time: 82.2 us; the launch traced here: 82 us
  Pallas kernels  79.8 us (97%)
  local copies, waits for them, and re-layouts  1.59 us (2%)
    pallas_call x1, Pallas kernels, fused(): pl.pallas_call(fused_kernel, out_shape=(shape, shape), in_specs=[local_sp...  79.8 us

profile of v3, /device:TPU:8, one launch (start us, length us, event | category | flops | bytes accessed | tf_op | source)
XLA Modules:
  0.0 82.0 jit_solution(11483896148906712479)
XLA Ops:
  0.6 79.8 %fused.1 = (bf16[128,2048]{1,0:T(8,128)(2,1)S(1)}, bf16[128,2048]{1,0:T(8,128)(2,1)S(1)}) custom-call(bf16[128,2048]{1,0:T(8,128)(2,1)} %mixer_tokens.1, bf16[2048]{0:T(1024)(128)(2,1)} %mixer_gain.1, bf16[2048,512]{1,0:T(8,128)(2,1)} %in_weight.1, bf16[1,512,512]{2,1,0:T(8,128)(2,1)} %group_weight.1, bf16[512]{0:T(512)(128)(2,1)} %channel_scale.1, ...), custom_call_target="tpu_custom_call" | custom-call | tf_op jit(solution)/shard_map/fused/pallas_call | solution.py:936
  80.4 0.8 copy.17
  81.2 0.8 copy.18

commit v4 on v3

--- a/solution.py
+++ b/solution.py
@@ -169,13 +169,14 @@
 MESH = pl.DeviceIdType.MESH
 GU_CUTS = (0, 1, 2, 4, 6, 8, 10, 12, 14, 16)
 PIECES_GU = len(GU_CUTS) - 1
-D_CUTS = (0, 2, 4, 6, 7, 8)
+D_CUTS = (0, 2, 4, 5, 6, 8)
 PIECES = PIECES_GU + len(D_CUTS) - 1
+X_PIECES = PIECES + 1
+Y_PIECES = PIECES - 1
 WINDOW = 5
 LAG = 3
 HALVES = 2
-CUTS = ((0, 1, 2, 4, 6, 8), (0, 2, 4, 6, 7, 8))
-CHUNKS = len(CUTS[0]) - 1
+CHUNKS = 8
 
 
 def fused_kernel(
@@ -277,8 +278,17 @@
         )
 
     barrier = pltpu.get_barrier_semaphore()
-    greet = [dev_c, dev_x, dev_y] + [(g, lax.rem(e + k, blocks), t) for k in range(1, blocks)]
-    for dev in greet:
+    for dev in (dev_c, dev_x, dev_y):
+        pl.semaphore_signal(barrier, inc=1, device_id=dev, device_id_type=MESH)
+
+    @pl.when(e < last)
+    def _():
+        dev = (g, lax.rem(e + 1, blocks), t)
+        pl.semaphore_signal(barrier, inc=1, device_id=dev, device_id_type=MESH)
+
+    @pl.when(e > 0)
+    def _():
+        dev = (g, lax.rem(e - 1 + blocks, blocks), t)
         pl.semaphore_signal(barrier, inc=1, device_id=dev, device_id_type=MESH)
 
     def loads():
@@ -288,7 +298,8 @@
             lane = pl.multiple_of(hh * ff_half, ff_half)
             out.append((gate_weight.at[0, :, pl.ds(lane, ff_half)], w_gu.at[t, hh, :, pl.ds(0, ff_half)]))
             out.append((up_weight.at[0, :, pl.ds(lane, ff_half)], w_gu.at[t, hh, :, pl.ds(ff_half, ff_half)]))
-        out.append((expert_tokens, exp_raw))
+            if h == 0:
+                out.append((expert_tokens, exp_raw))
         out.append((down_weight.at[0], w_d.at[t]))
         out.append((mixer_tokens, mix_raw))
         out.append((in_weight, w_in))
@@ -300,7 +311,7 @@
     for copy in local:
         copy.start()
     def norm(raw, gain, dst, start, count):
-        step = 16
+        step = 32
         gain_row = gain[...].astype(f32).reshape(1, width)
 
         @pl.loop(0, count // step)
@@ -310,8 +321,6 @@
             scaled = values * lax.rsqrt(jnp.mean(values * values, axis=-1, keepdims=True) + 1e-06)
             dst[at, :] = (scaled * gain_row).astype(bf16)
 
-    local[4].wait()
-    norm(exp_raw, expert_gain, tokens.at[e], 0, rows)
     ids = route_ids[...]
     weights = route_weights[...]
     shares = weights / jnp.sum(weights, axis=0, keepdims=True)
@@ -334,37 +343,45 @@
         start, n = d_cut(s)
         return w_d.at[q, pl.ds(pl.multiple_of(h * ff_half + start, 16), n), :]
 
+    def x_piece(q, s):
+        return piece(q, g, s) if s < PIECES else piece(q, 1 - g, PIECES - 1)
+
+    def kind(s):
+        return 0 if s < PIECES_GU else 1
+
     def send_x(s):
-        p = piece(t, g, s)
-        return rc(p, p, x_send.at[s], x_recv.at[s], dev_x)
+        p = x_piece(t, s)
+        return rc(p, p, x_send.at[kind(s)], x_recv.at[s], dev_x)
 
     def got_x(s):
-        p = piece(t_x, g, s)
-        return rc(p, p, x_send.at[s], x_recv.at[s], dev_x)
+        p = x_piece(t_x, s)
+        return rc(p, p, x_send.at[0], x_recv.at[s], dev_x)
 
     def send_y(s):
         p = piece(t_x, g, s)
-        return rc(p, p, y_send.at[s], y_recv.at[s], dev_y)
+        return rc(p, p, y_send.at[kind(s)], y_recv.at[s], dev_y)
 
     def got_y(s):
         p = piece(t_x, 1 - g, s)
-        return rc(p, p, y_send.at[s], y_recv.at[s], dev_y)
+        return rc(p, p, y_send.at[0], y_recv.at[s], dev_y)
 
     def send_fx(s):
-        p = piece(t_x, g, s)
-        return rc(p, p, fx_send.at[s], fx_recv.at[s], dev_c)
-
-    def got_fx(s):
-        p = piece(t_d, g, s)
-        return rc(p, p, fx_send.at[s], fx_recv.at[s], dev_c)
+        p = x_piece(t_x, s)
+        return rc(p, p, fx_send.at[kind(s)], fx_recv.at[kind(s)], dev_c)
 
     def send_fy(s):
         p = piece(t_x, 1 - g, s)
-        return rc(p, p, fy_send.at[s], fy_recv.at[s], dev_c)
-
-    def got_fy(s):
-        p = piece(t_d, 1 - g, s)
-        return rc(p, p, fy_send.at[s], fy_recv.at[s], dev_c)
+        return rc(p, p, fy_send.at[kind(s)], fy_recv.at[kind(s)], dev_c)
+
+    d_last = d_cut(PIECES - 1)
+    x_rows, y_rows = ff_half + d_last[1], d_last[0]
+
+    def all_gu(send, recv):
+        return rc(w_gu.at[t, g], w_gu.at[t, g], send.at[0], recv.at[0], dev_c)
+
+    def all_d(send, recv, count):
+        p = w_d.at[t, pl.ds(0, count), :]
+        return rc(p, p, send.at[1], recv.at[1], dev_c)
 
     def own_gu(q):
         return rc(w_gu.at[q], w_gu.at[q], own_send.at[0], own_recv.at[0], dev_c)
@@ -377,11 +394,11 @@
 
     def ag_far(home, j, f):
         p = chunk(home, j)
-        return rc(p, p, ag_send.at[f], ag_recv.at[f + 6 * (1 - u)], far)
+        return rc(p, p, ag_send.at[0], ag_recv.at[f + 6 * (1 - u)], far)
 
     def ag_near(home, j, f):
         p = chunk(home, j)
-        return rc(p, p, ag_send.at[4 + f], ag_recv.at[f], near)
+        return rc(p, p, ag_send.at[1], ag_recv.at[f], near)
 
     def ag_got(home, j, f):
         p = chunk(home, j)
@@ -397,13 +414,14 @@
         dev = ((g, lax.rem(e + 1, blocks), t), dev_x, dev_c)[k]
         return rc(src, rim_rows, rim_send.at[k], rim_recv.at[k], dev)
 
-    def coef_to(k):
-        dev = (g, lax.rem(e + k, blocks), t)
-        return rc(coefs.at[e], coefs.at[e], coef_send.at[k - 1], coef_recv.at[k - 1], dev)
-
-    def coef_got(k):
-        home = lax.rem(e - k + blocks, blocks)
-        return rc(coefs.at[home], coefs.at[home], coef_send.at[k - 1], coef_recv.at[k - 1], dev_c)
+    def coef_far(home, k):
+        return rc(coefs.at[home], coefs.at[home], coef_send.at[0], coef_recv.at[k + 3 * (1 - u)], far)
+
+    def coef_near(home, k):
+        return rc(coefs.at[home], coefs.at[home], coef_send.at[1], coef_recv.at[k], near)
+
+    def coef_got(home, k):
+        return rc(coefs.at[home], coefs.at[home], coef_send.at[0], coef_recv.at[k], far)
 
     def d2_half(ref, q, h):
         return ref.at[q, pl.ds(pl.multiple_of(h * ff_half, ff_half), ff_half), :]
@@ -416,56 +434,63 @@
         return rc(d2_half(w_d, t, g), d2_half(w_d2, t, g), d2_send.at[0], d2_recv.at[0], far)
 
     def d2_relay(s):
-        k = 1 + s - PIECES_GU
-        return rc(d2_piece(w_d, s), d2_piece(w_d2, s), d2_send.at[k], d2_recv.at[k], far)
-
-    def d2_hid(xq, k):
-        return rc(hid.at[third, xq], hid_far.at[xq], d2_send.at[6 + k], d2_recv.at[6 + k], far)
+        return rc(d2_piece(w_d, s), d2_piece(w_d2, s), d2_send.at[1], d2_recv.at[1], far)
+
+    def d2_hid(xq):
+        return rc(hid.at[third, xq], hid_far.at[xq], d2_send.at[2], d2_recv.at[2], far)
 
     def d2_y(k, mine):
         p = d2_half(w_d2, t if k == 0 else t_x, g if mine else 1 - g)
-        return rc(p, p, d2_send.at[8 + k], d2_recv.at[8 + k], dev_y)
-
-    def d2_c(k, mine):
-        q = (t if k % 2 == 0 else t_x) if mine else (t_c if k % 2 == 0 else t_d)
-        p = d2_half(w_d2, q, g if k < 2 else 1 - g)
-        return rc(p, p, d2_send.at[10 + k], d2_recv.at[10 + k], dev_c)
+        return rc(p, p, d2_send.at[3], d2_recv.at[3 + k], dev_y)
+
+    def d2_c(k):
+        p = d2_half(w_d2, t if k % 2 == 0 else t_x, g if k < 2 else 1 - g)
+        return rc(p, p, d2_send.at[4], d2_recv.at[5], dev_c)
+
+    def d2_all(k, p):
+        return rc(p, p, d2_send.at[k], d2_recv.at[min(k, 2) if k < 4 else 5], dev_c)
 
     def mix_x(q, j):
         p = mix_all.at[q, pl.ds(j * half_rows, half_rows), :]
-        return rc(p, p, mix_send.at[j], mix_recv.at[j], dev_x)
+        return rc(p, p, mix_send.at[0], mix_recv.at[j], dev_x)
 
     def mix_fwd(q, j):
         p = mix_all.at[q, pl.ds(j * half_rows, half_rows), :]
-        return rc(p, p, mix_send.at[2 + j], mix_recv.at[2 + j], dev_c)
+        return rc(p, p, mix_send.at[1], mix_recv.at[2], dev_c)
 
     def mix_own(q):
-        return rc(mix_all.at[q], mix_all.at[q], mix_send.at[4], mix_recv.at[4], dev_c)
+        return rc(mix_all.at[q], mix_all.at[q], mix_send.at[2], mix_recv.at[3], dev_c)
 
     local[0].wait()
     local[1].wait()
-    pl.semaphore_wait(barrier, len(greet))
+    @pl.when(end)
+    def _():
+        pl.semaphore_wait(barrier, 4)
+
+    @pl.when(mid)
+    def _():
+        pl.semaphore_wait(barrier, 5)
+
     for s in range(WINDOW):
         send_x(s).start()
-    for k in range(1, blocks):
-        coef_to(k).start()
+    local[2].wait()
+    norm(exp_raw, expert_gain, tokens.at[e], 0, rows)
     for j in range(HALVES):
         ag_far(e, j, j).start()
-
-        @pl.when(mid)
-        def _():
+    coef_far(e, 0).start()
+
+    @pl.when(mid)
+    def _():
+        for j in range(HALVES):
             ag_near(e, j, j).start()
-
-    local[2].wait()
+        coef_near(e, 0).start()
+
     local[3].wait()
+    local[4].wait()
     own_gu(t).start()
     local[5].wait()
     own_d(t).start()
 
-    @pl.when(end)
-    def _():
-        d2_own().start()
-
     local[6].wait()
     norm(mix_raw, mixer_gain, mix_all.at[t], 0, rows)
 
@@ -473,31 +498,38 @@
     def _():
         rim_to(0).start()
 
+    @pl.when(end)
+    def _():
+        d2_own().start()
+
     mix_own(t).start()
 
-    def hidden(home, xq):
+    whole = pl.ds(0, rows)
+    part_of = [pl.ds(j * half_rows, half_rows) for j in range(HALVES)]
+
+    def hidden(home, xq, at=whole):
         @pl.loop(0, 4)
         def _(j):
             q = 2 * xq + j // 2
             h = j % 2
-            both = jnp.dot(tokens[home], w_gu[q, h], preferred_element_type=f32)
+            both = jnp.dot(tokens[home, at, :], w_gu[q, h], preferred_element_type=f32)
             gate, upper = both[:, :ff_half], both[:, ff_half:]
             value = gate / (1.0 + jnp.exp(-gate)) * upper
-            hid[home, xq, :, pl.ds(pl.multiple_of(j * ff_half, ff_half), ff_half)] = value.astype(bf16)
+            hid[home, xq, at, pl.ds(pl.multiple_of(j * ff_half, ff_half), ff_half)] = value.astype(bf16)
 
     col = 512
 
-    def down(home, xq, first):
+    def down(home, xq, first, at=whole):
         @pl.loop(0, width // col)
         def _(n):
-            at = pl.ds(pl.multiple_of(n * col, col), col)
-            w = w_d[pl.ds(2 * xq, 2), :, at].reshape(4 * ff_half, col)
-            part = jnp.dot(hid[home, xq], w, preferred_element_type=f32)
+            cols = pl.ds(pl.multiple_of(n * col, col), col)
+            w = w_d[pl.ds(2 * xq, 2), :, cols].reshape(4 * ff_half, col)
+            part = jnp.dot(hid[home, xq, at, :], w, preferred_element_type=f32)
             if first:
-                acc[home, :, at] = part
+                acc[home, at, cols] = part
             else:
-                scale = scales[home][:, :1]
-                acc[home, :, at] = (acc[home, :, at] + part) * scale
+                scale = scales[home, at, :][:, :1]
+                acc[home, at, cols] = (acc[home, at, cols] + part) * scale
 
     def pool_in(xq):
         @pl.loop(0, 2)
@@ -507,9 +539,8 @@
             pooled_in[pl.ds(pl.multiple_of(rows * (q + 1), rows), rows), :] = value.astype(bf16)
 
     def wait_fgu():
-        for s in range(PIECES_GU):
-            got_fx(s).wait_recv()
-            got_fy(s).wait_recv()
+        all_gu(fx_send, fx_recv).wait_recv()
+        all_gu(fy_send, fy_recv).wait_recv()
 
     def relay_y(s):
         got_y(s).wait_recv()
@@ -518,7 +549,10 @@
     def gather(f):
         @pl.when(end)
         def _():
-            ag_got(mirror(1 + f // 2), f % 2, f).wait_recv()
+            home = mirror(1 + f // 2)
+            ag_got(home, f % 2, f).wait_recv()
+            if f % 2 == 1:
+                coef_got(home, f // 2).wait_recv()
 
         if f < 4:
 
@@ -527,6 +561,9 @@
                 home = mirror(2 + f // 2)
                 ag_got(home, f % 2, f).wait_recv()
                 ag_near(home, f % 2, f + 2).start()
+                if f % 2 == 1:
+                    coef_got(home, f // 2).wait_recv()
+                    coef_near(home, f // 2 + 1).start()
 
         if f < 2:
 
@@ -535,41 +572,42 @@
                 home = mirror(0)
                 ag_got(home, f % 2, 6 + f).wait_recv()
                 ag_far(home, f % 2, 2 + f).start()
-
-    for s in range(PIECES):
+                if f % 2 == 1:
+                    coef_got(home, 3).wait_recv()
+                    coef_far(home, 1).start()
+
+    def scale_of(home):
+        scales[home] = jnp.transpose(jnp.broadcast_to(coefs[home, pl.ds(e, 1), :], (rows, rows)))
+
+    for s in range(X_PIECES):
         got_x(s).wait_recv()
-        send_y(s).start()
+        if s < Y_PIECES:
+            send_y(s).start()
         send_fx(s).start()
-        if s >= PIECES_GU:
+        if PIECES_GU <= s < PIECES:
 
             @pl.when(end)
             def _():
                 d2_relay(s).start()
 
-        if s + WINDOW == PIECES:
+        if s + WINDOW == X_PIECES:
 
             @pl.when(rim_mine)
             def _():
                 rim_to(1).start()
 
-        if s + WINDOW < PIECES:
+        if s + WINDOW < X_PIECES:
             send_x(s + WINDOW).start()
-        elif s + WINDOW < PIECES + HALVES:
-            mix_x(t, s + WINDOW - PIECES).start()
+        elif s + WINDOW < X_PIECES + HALVES:
+            mix_x(t, s + WINDOW - X_PIECES).start()
         if s >= LAG:
             relay_y(s - LAG)
         if s in (3, 5, 7, 9, 11):
             gather(s // 2 - 1)
-        if s == 2:
-            for k in range(1, blocks):
-                coef_got(k).wait_recv()
-            for home in range(blocks):
-                row = coefs[home, pl.ds(e, 1), :]
-                scales[home] = jnp.transpose(jnp.broadcast_to(row, (rows, rows)))
         if s == 3:
             own_gu(t_c).wait_recv()
             hidden(e, x)
-        if s == 6:
+        if s == 8:
 
             @pl.when(rim_mine)
             def _():
@@ -586,7 +624,7 @@
 
             @pl.when(end)
             def _():
-                d2_hid(x, 0).start()
+                d2_hid(x).start()
 
         if s == 7:
 
@@ -602,56 +640,57 @@
             hidden(mirror(2), x)
             down(mirror(2), x, True)
         if s == 11:
+            hidden(mirror(3), x, part_of[0])
+        if s == 12:
             wait_fgu()
             hidden(third, 1 - x)
 
             @pl.when(end)
             def _():
-                d2_hid(1 - x, 1).start()
-
+                d2_hid(1 - x).start()
+
+        if s == Y_PIECES:
+
+            @pl.when(mid)
+            def _():
+                d2_own().wait_recv()
+                d2_y(0, True).start()
+                d2_c(0).start()
+
+            hidden(mirror(3), 1 - x, part_of[0])
+
+    for s in range(X_PIECES - LAG, Y_PIECES):
+        relay_y(s)
+    down(mirror(3), x, True, part_of[0])
     gather(5)
-    hidden(mirror(3), x)
-    relay_y(PIECES - 3)
-    down(mirror(3), x, True)
-    relay_y(PIECES - 2)
-    hidden(mirror(3), 1 - x)
-    relay_y(PIECES - 1)
-
-    @pl.when(mid)
-    def _():
-        d2_own().wait_recv()
-        d2_y(0, True).start()
-        d2_c(0, True).start()
-
-    for s in range(PIECES_GU, PIECES):
-        got_fx(s).wait_recv()
-        got_fy(s).wait_recv()
+    for home in range(blocks):
+        scale_of(home)
+    all_d(fx_send, fx_recv, x_rows).wait_recv()
+    all_d(fy_send, fy_recv, y_rows).wait_recv()
 
     def cut(k):
         slot, j = divmod(k, CHUNKS)
-        unit = rows // CUTS[slot][-1]
-        low, high = CUTS[slot][j], CUTS[slot][j + 1]
-        return slot, pl.ds(low * unit, (high - low) * unit)
+        return slot, pl.ds(j * (rows // CHUNKS), rows // CHUNKS)
 
     def rs_far(k):
         slot, at = cut(k)
         sem = k + 2 * CHUNKS * u
-        return rc(rs_stage.at[slot, at, :], rs_in.at[slot + 2 * u, at, :], rs_send.at[k], rs_recv.at[sem], far)
+        return rc(rs_stage.at[slot, at, :], rs_in.at[slot + 2 * u, at, :], rs_send.at[0], rs_recv.at[sem], far)
 
     def rs_near(k):
         slot, at = cut(k)
         sem = 2 * CHUNKS + k
-        return rc(rs_stage.at[2, at, :], rs_in.at[2, at, :], rs_send.at[sem], rs_recv.at[sem], near)
+        return rc(rs_stage.at[2, at, :], rs_in.at[2, at, :], rs_send.at[1], rs_recv.at[sem], near)
 
     def rs_got(k, base):
         slot, at = cut(k)
         p = rs_in.at[slot + base, at, :]
         return rc(p, p, rs_send.at[0], rs_recv.at[k + base * CHUNKS], far)
 
-    def first_send(home, first):
+    def first_send(home, first, count=CHUNKS):
         @pl.when(end)
         def _():
-            for k in range(first, first + CHUNKS):
+            for k in range(first, first + count):
                 slot, at = cut(k)
                 rs_stage[slot, at, :] = acc[home, at, :].astype(bf16)
                 rs_far(k).start()
@@ -697,11 +736,11 @@
             mix_part[j, :, at] = jnp.dot(grouped, w_out[:, at], preferred_element_type=f32).astype(bf16)
 
     def pair_to(j):
-        return rc(mix_part.at[2 * j], mix_pair.at[j], mix_send.at[6 + j], mix_recv.at[6 + j], dev_c)
+        return rc(mix_part.at[2 * j], mix_pair.at[j], mix_send.at[3], mix_recv.at[4 + j], dev_c)
 
     def cross(j):
         at = pl.ds(j * half_rows, half_rows)
-        return rc(mix_stage.at[at, :], mix_far.at[at, :], mix_send.at[8 + j], mix_recv.at[8 + j], dev_x)
+        return rc(mix_stage.at[at, :], mix_far.at[at, :], mix_send.at[4], mix_recv.at[6 + j], dev_x)
 
     def mix_relay(j):
         mix_x(t_x, j).wait_recv()
@@ -719,32 +758,43 @@
             rs_got(k, 2).wait_recv()
             expert_out[at, :] = (acc[e, at, :] + rs_in[2, at, :].astype(f32)).astype(bf16)
 
-    down(mirror(3), 1 - x, False)
-    first_send(mirror(3), 0)
+    down(mirror(3), 1 - x, False, part_of[0])
+    first_send(mirror(3), 0, CHUNKS // 2)
+    hidden(mirror(3), x, part_of[1])
+    hidden(mirror(3), 1 - x, part_of[1])
+    lead(0)
+    down(mirror(3), x, True, part_of[1])
+    lead(1)
+    down(mirror(3), 1 - x, False, part_of[1])
+    first_send(mirror(3), CHUNKS // 2, CHUNKS // 2)
+
+    @pl.when(mid)
+    def _():
+        d2_all(1, d2_half(w_d2, t_x, g)).wait_recv()
+        d2_y(1, True).start()
+        d2_c(1).start()
+
+    mix_relay(0)
+    lead(2)
     hidden(mirror(2), 1 - x)
-    lead(0)
+
+    @pl.when(rim_relay)
+    def _():
+        rim_to(1).wait_recv()
+        rim_to(2).start()
+
+    lead(3)
     down(mirror(2), 1 - x, False)
     first_send(mirror(2), CHUNKS)
-    mix_relay(0)
-    lead(1)
+    lead(4)
+    mix_relay(1)
 
     @pl.when(mid)
     def _():
         down(third, 1 - x, False)
-        for s in range(PIECES_GU, PIECES):
-            d2_relay(s).wait_recv()
-        d2_y(1, True).start()
-        d2_c(1, True).start()
-
-    @pl.when(rim_relay)
-    def _():
-        rim_to(1).wait_recv()
-        rim_to(2).start()
-
-    mix_relay(1)
-    lead(2)
-    for j in range(HALVES):
-        mix_fwd(t_d, j).wait_recv()
+
+    mix_all_in = rc(mix_all.at[t_d], mix_all.at[t_d], mix_send.at[1], mix_recv.at[2], dev_c)
+    mix_all_in.wait_recv()
     pool_in(1 - x)
 
     @pl.when(rim_last)
@@ -756,53 +806,57 @@
         value = jnp.dot(rim_rows[...], w_in[...], preferred_element_type=f32)
         pooled_in[pl.ds(rows - rim_rows.shape[0], rim_rows.shape[0]), :] = value.astype(bf16)
 
+    lead(5)
+    lag(0)
     mix_down(0)
     pair_to(0).start()
-    lead(3)
+    lead(6)
+    lag(1)
     mix_down(1)
+    lead(7)
+    lag(2)
     pair_to(0).wait_recv()
     for j in range(HALVES):
         at = pl.ds(j * half_rows, half_rows)
         mix_stage[at, :] = (mix_part[1, at, :].astype(f32) + mix_pair[0, at, :].astype(f32)).astype(bf16)
         cross(j).start()
-    lag(0)
-    lag(1)
-    lag(2)
-    lead(4)
+    lead(8)
+    lag(3)
+
+    hidden(e, 1 - x)
+    lead(9)
+    lag(4)
 
     @pl.when(mid)
     def _():
         d2_y(0, False).wait_recv()
-        d2_c(2, True).start()
-
-    lag(3)
-    hidden(e, 1 - x)
-    lead(5)
+        d2_c(2).start()
+
     down(e, 1 - x, False)
-    lag(4)
+    lead(10)
+    lag(5)
+    lead(11)
+    lag(6)
     mix_down(2)
     pair_to(1).start()
-    lead(6)
-    lag(5)
+    lead(12)
+    lag(7)
+    lead(13)
     mix_down(3)
-    lead(7)
-    lag(6)
+    lead(14)
 
     @pl.when(mid)
     def _():
         d2_y(1, False).wait_recv()
-        d2_c(3, True).start()
-
-    lead(8)
-    lead(9)
+        d2_c(3).start()
+
+    lead(15)
 
     @pl.when(mid)
     def _():
         scales[0] = jnp.transpose(jnp.broadcast_to(coefs[e, pl.ds(mirror(0), 1), :], (rows, rows)))
-        d2_hid(x, 0).wait_recv()
-        d2_hid(1 - x, 1).wait_recv()
-        for k in range(4):
-            d2_c(k, False).wait_recv()
+        d2_all(2, hid_far).wait_recv()
+        d2_all(4, w_d2.at[pl.ds(0, 2)]).wait_recv()
 
         @pl.loop(0, width // col)
         def _(n):
@@ -814,10 +868,9 @@
                 part = part + jnp.dot(hid_far[xq], w, preferred_element_type=f32) * scale
             acc[e, :, at] = part
 
-    final(0)
-    final(1)
-    lag(7)
-    final(2)
+    for k in range(4):
+        lag(CHUNKS + k)
+        final(k)
     pair_to(1).wait_recv()
     for j in range(HALVES):
         at = pl.ds(j * half_rows, half_rows)
@@ -825,22 +878,26 @@
         mixed_out[at, :] = (
             mix_part[3, at, :].astype(f32) + mix_pair[1, at, :].astype(f32) + mix_far[at, :].astype(f32)
         ).astype(bf16)
-    for s in range(PIECES):
-        send_x(s).wait_send()
-        send_y(s).wait_send()
-        send_fx(s).wait_send()
-        send_fy(s).wait_send()
+
+    all_gu(x_send, fx_recv).wait_send()
+    all_d(x_send, fx_recv, x_rows).wait_send()
+    all_gu(y_send, fx_recv).wait_send()
+    all_d(y_send, fx_recv, y_rows).wait_send()
+    all_gu(fx_send, fx_recv).wait_send()
+    all_d(fx_send, fx_recv, x_rows).wait_send()
+    all_gu(fy_send, fx_recv).wait_send()
+    all_d(fy_send, fx_recv, y_rows).wait_send()
     own_gu(t).wait_send()
     own_d(t).wait_send()
-    for k in range(1, blocks):
-        coef_to(k).wait_send()
-    for j in range(HALVES):
-        ag_far(e, j, j).wait_send()
-        mix_x(t, j).wait_send()
-        mix_fwd(t_x, j).wait_send()
-        pair_to(j).wait_send()
-        cross(j).wait_send()
-    mix_own(t).wait_send()
+
+    def sent(sems, k, p):
+        rc(p, p, sems.at[k], mix_recv.at[0], dev_c).wait_send()
+
+    sent(mix_send, 0, mix_all.at[t])
+    sent(mix_send, 1, mix_all.at[t])
+    sent(mix_send, 2, mix_all.at[t])
+    sent(mix_send, 3, mix_part.at[pl.ds(0, 2)])
+    sent(mix_send, 4, mix_stage)
 
     @pl.when(rim_source)
     def _():
@@ -857,34 +914,26 @@
 
     @pl.when(end)
     def _():
+        sent(ag_send, 0, tokens.at[e])
+        sent(coef_send, 0, coefs.at[e])
         d2_own().wait_send()
-        d2_hid(x, 0).wait_send()
-        d2_hid(1 - x, 1).wait_send()
-        for s in range(PIECES_GU, PIECES):
-            d2_relay(s).wait_send()
+        sent(d2_send, 1, d2_half(w_d, t_x, g))
+        sent(d2_send, 2, hid_far)
 
     @pl.when(mid)
     def _():
-        for f in range(6):
-            ag_near(e, f % 2, f).wait_send()
-        for f in range(2):
-            ag_far(e, f, 2 + f).wait_send()
-        for k in range(2):
-            d2_y(k, True).wait_send()
-        for k in range(4):
-            d2_c(k, True).wait_send()
-
-    lag(8)
-    final(3)
-    lag(9)
-    final(4)
-    for k in range(2 * CHUNKS):
-        rs_far(k).wait_send()
-
-    @pl.when(mid)
-    def _():
-        for k in range(CHUNKS):
-            rs_near(k).wait_send()
+        sent(ag_send, 0, tokens.at[pl.ds(0, 2)])
+        sent(ag_send, 1, tokens.at[pl.ds(0, 3)])
+        sent(coef_send, 0, coefs.at[pl.ds(0, 2)])
+        sent(coef_send, 1, coefs.at[pl.ds(0, 3)])
+        sent(d2_send, 3, w_d2.at[0])
+        sent(d2_send, 4, w_d2.at[pl.ds(0, 2)])
+        sent(rs_send, 1, rs_stage.at[2])
+
+    for k in range(4, CHUNKS):
+        lag(CHUNKS + k)
+        final(k)
+    sent(rs_send, 0, rs_stage.at[pl.ds(0, 2)])
 
 
 def fused(*args):
@@ -930,7 +979,7 @@
         vmem((2, rows, 2 * ff), bf16),
         dma((10,)),
     ]
-    for count in (PIECES, PIECES, PIECES, PIECES, 2, 2, PIECES, PIECES, PIECES, PIECES, 10, 8, 3, 3, 3 * CHUNKS, 4 * CHUNKS, 10, 10, 3, 3, 14, 14):
+    for count in (2, X_PIECES, 2, Y_PIECES, 2, 2, 2, 2, 2, 2, 2, 8, 2, 4, 2, 4 * CHUNKS, 5, 8, 3, 3, 5, 6):
         scratch.append(dma((count,)))
     shape = vmem((rows, width), bf16)
     return pl.pallas_call(

time: 82.2 us -> 78.4 us (0.954)
  Pallas kernels: 79.8 us -> 75.8 us
    pallas_call x1, Pallas kernels: 79.8 us -> 75.8 us  [fused(): pl.pallas_call(fused_kernel, out_shape=(shape, shape), in_specs=[local_sp...]
where the time goes in v4:
time: 78.4 us; the launch traced here: 78 us
  Pallas kernels  75.8 us (97%)
  local copies, waits for them, and re-layouts  1.59 us (2%)
    pallas_call x1, Pallas kernels, fused(): pl.pallas_call(fused_kernel, out_shape=(shape, shape), in_specs=[local_sp...  75.8 us
    unnamed x2, local copies, waits for them, and re-layouts  1.59 us

profile of v4, /device:TPU:8, one launch (start us, length us, event | category | flops | bytes accessed | tf_op | source)
XLA Modules:
  0.0 78.0 jit_solution(686769029649098136)
XLA Ops:
  0.6 75.8 %fused.1 = (bf16[128,2048]{1,0:T(8,128)(2,1)S(1)}, bf16[128,2048]{1,0:T(8,128)(2,1)S(1)}) custom-call(bf16[128,2048]{1,0:T(8,128)(2,1)} %mixer_tokens.1, bf16[2048]{0:T(1024)(128)(2,1)} %mixer_gain.1, bf16[2048,512]{1,0:T(8,128)(2,1)} %in_weight.1, bf16[1,512,512]{2,1,0:T(8,128)(2,1)} %group_weight.1, bf16[512]{0:T(512)(128)(2,1)} %channel_scale.1, ...), custom_call_target="tpu_custom_call" | custom-call | tf_op jit(solution)/shard_map/fused/pallas_call | solution.py:985
  76.4 0.8 %copy.17 = bf16[128,2048]{1,0:T(8,128)(2,1)} copy(bf16[128,2048]{1,0:T(8,128)(2,1)S(1)} %get-tuple-element.2) | data formatting | bytes 1048576
  77.2 0.8 %copy.18 = bf16[128,2048]{1,0:T(8,128)(2,1)} copy(bf16[128,2048]{1,0:T(8,128)(2,1)S(1)} %get-tuple-element.3) | data formatting | bytes 1048576

commit v5 on v4

--- a/solution.py
+++ b/solution.py
@@ -308,7 +308,7 @@
         return [pltpu.make_async_copy(a, b, load_sem.at[i]) for i, (a, b) in enumerate(out)]
 
     local = loads()
-    for copy in local:
+    for copy in local[:3]:
         copy.start()
     def norm(raw, gain, dst, start, count):
         step = 32
@@ -473,17 +473,19 @@
 
     for s in range(WINDOW):
         send_x(s).start()
+    for copy in local[3:]:
+        copy.start()
     local[2].wait()
     norm(exp_raw, expert_gain, tokens.at[e], 0, rows)
+    coef_far(e, 0).start()
     for j in range(HALVES):
         ag_far(e, j, j).start()
-    coef_far(e, 0).start()
 
     @pl.when(mid)
     def _():
+        coef_near(e, 0).start()
         for j in range(HALVES):
             ag_near(e, j, j).start()
-        coef_near(e, 0).start()
 
     local[3].wait()
     local[4].wait()
@@ -551,7 +553,7 @@
         def _():
             home = mirror(1 + f // 2)
             ag_got(home, f % 2, f).wait_recv()
-            if f % 2 == 1:
+            if f % 2 == 0:
                 coef_got(home, f // 2).wait_recv()
 
         if f < 4:
@@ -561,7 +563,7 @@
                 home = mirror(2 + f // 2)
                 ag_got(home, f % 2, f).wait_recv()
                 ag_near(home, f % 2, f + 2).start()
-                if f % 2 == 1:
+                if f % 2 == 0:
                     coef_got(home, f // 2).wait_recv()
                     coef_near(home, f // 2 + 1).start()
 
@@ -572,7 +574,7 @@
                 home = mirror(0)
                 ag_got(home, f % 2, 6 + f).wait_recv()
                 ag_far(home, f % 2, 2 + f).start()
-                if f % 2 == 1:
+                if f % 2 == 0:
                     coef_got(home, 3).wait_recv()
                     coef_far(home, 1).start()
 
@@ -658,13 +660,11 @@
                 d2_c(0).start()
 
             hidden(mirror(3), 1 - x, part_of[0])
+            down(mirror(3), x, True, part_of[0])
+            scale_of(mirror(3))
 
     for s in range(X_PIECES - LAG, Y_PIECES):
         relay_y(s)
-    down(mirror(3), x, True, part_of[0])
-    gather(5)
-    for home in range(blocks):
-        scale_of(home)
     all_d(fx_send, fx_recv, x_rows).wait_recv()
     all_d(fy_send, fy_recv, y_rows).wait_recv()
 
@@ -760,6 +760,9 @@
 
     down(mirror(3), 1 - x, False, part_of[0])
     first_send(mirror(3), 0, CHUNKS // 2)
+    gather(5)
+    for home in (mirror(2), third, e):
+        scale_of(home)
     hidden(mirror(3), x, part_of[1])
     hidden(mirror(3), 1 - x, part_of[1])
     lead(0)

time: 78.4 us -> 77.7 us (level)
  no operation moved by 1% of the time
where the time goes in v5:
time: 77.7 us; the launch traced here: 77.6 us
  Pallas kernels  75.3 us (97%)
  local copies, waits for them, and re-layouts  1.59 us (2%)
    pallas_call x1, Pallas kernels, fused(): pl.pallas_call(fused_kernel, out_shape=(shape, shape), in_specs=[local_sp...  75.3 us
    unnamed x2, local copies, waits for them, and re-layouts  1.59 us

profile of v5, /device:TPU:8, one launch (start us, length us, event | category | flops | bytes accessed | tf_op | source)
XLA Modules:
  0.0 77.6 jit_solution(4285424787516146776)
XLA Ops:
  0.6 75.3 %fused.1 = (bf16[128,2048]{1,0:T(8,128)(2,1)S(1)}, bf16[128,2048]{1,0:T(8,128)(2,1)S(1)}) custom-call(bf16[128,2048]{1,0:T(8,128)(2,1)} %mixer_tokens.1, bf16[2048]{0:T(1024)(128)(2,1)} %mixer_gain.1, bf16[2048,512]{1,0:T(8,128)(2,1)} %in_weight.1, bf16[1,512,512]{2,1,0:T(8,128)(2,1)} %group_weight.1, bf16[512]{0:T(512)(128)(2,1)} %channel_scale.1, ...), custom_call_target="tpu_custom_call" | custom-call | tf_op jit(solution)/shard_map/fused/pallas_call | solution.py:988
  76.0 0.8 %copy.17 = bf16[128,2048]{1,0:T(8,128)(2,1)} copy(bf16[128,2048]{1,0:T(8,128)(2,1)S(1)} %get-tuple-element.2) | data formatting | bytes 1048576
  76.8 0.8 %copy.18 = bf16[128,2048]{1,0:T(8,128)(2,1)} copy(bf16[128,2048]{1,0:T(8,128)(2,1)S(1)} %get-tuple-element.3) | data formatting | bytes 1048576

commit v6 on v5

--- a/solution.py
+++ b/solution.py
@@ -519,7 +519,7 @@
             value = gate / (1.0 + jnp.exp(-gate)) * upper
             hid[home, xq, at, pl.ds(pl.multiple_of(j * ff_half, ff_half), ff_half)] = value.astype(bf16)
 
-    col = 512
+    col = 2 * width * HALVES // CHUNKS
 
     def down(home, xq, first, at=whole):
         @pl.loop(0, width // col)

time: 77.7 us -> 77.6 us (level)
  no operation moved by 1% of the time
where the time goes in v6:
time: 77.6 us; the launch traced here: 77.4 us
  Pallas kernels  75.2 us (97%)
  local copies, waits for them, and re-layouts  1.59 us (2%)
    pallas_call x1, Pallas kernels, fused(): pl.pallas_call(fused_kernel, out_shape=(shape, shape), in_specs=[local_sp...  75.2 us
    unnamed x2, local copies, waits for them, and re-layouts  1.59 us

profile of v6, /device:TPU:8, one launch (start us, length us, event | category | flops | bytes accessed | tf_op | source)
XLA Modules:
  0.0 77.4 jit_solution(14597021845668054552)
XLA Ops:
  0.6 75.2 %fused.1 = (bf16[128,2048]{1,0:T(8,128)(2,1)S(1)}, bf16[128,2048]{1,0:T(8,128)(2,1)S(1)}) custom-call(bf16[128,2048]{1,0:T(8,128)(2,1)} %mixer_tokens.1, bf16[2048]{0:T(1024)(128)(2,1)} %mixer_gain.1, bf16[2048,512]{1,0:T(8,128)(2,1)} %in_weight.1, bf16[1,512,512]{2,1,0:T(8,128)(2,1)} %group_weight.1, bf16[512]{0:T(512)(128)(2,1)} %channel_scale.1, ...), custom_call_target="tpu_custom_call" | custom-call | tf_op jit(solution)/shard_map/fused/pallas_call | solution.py:988
  75.8 0.8 %copy.17 = bf16[128,2048]{1,0:T(8,128)(2,1)} copy(bf16[128,2048]{1,0:T(8,128)(2,1)S(1)} %get-tuple-element.2) | data formatting | bytes 1048576
  76.6 0.8 %copy.18 = bf16[128,2048]{1,0:T(8,128)(2,1)} copy(bf16[128,2048]{1,0:T(8,128)(2,1)S(1)} %get-tuple-element.3) | data formatting | bytes 1048576

commit v7 on v5

--- a/solution.py
+++ b/solution.py
@@ -311,7 +311,7 @@
     for copy in local[:3]:
         copy.start()
     def norm(raw, gain, dst, start, count):
-        step = 32
+        step = 64
         gain_row = gain[...].astype(f32).reshape(1, width)
 
         @pl.loop(0, count // step)

time: 77.7 us -> 77.7 us (level)
  no operation moved by 1% of the time
where the time goes in v7:
time: 77.7 us; the launch traced here: 77.6 us
  Pallas kernels  75.3 us (97%)
  local copies, waits for them, and re-layouts  1.59 us (2%)
    pallas_call x1, Pallas kernels, fused(): pl.pallas_call(fused_kernel, out_shape=(shape, shape), in_specs=[local_sp...  75.3 us
    unnamed x2, local copies, waits for them, and re-layouts  1.59 us

profile of v7, /device:TPU:8, one launch (start us, length us, event | category | flops | bytes accessed | tf_op | source)
XLA Modules:
  0.0 77.6 jit_solution(5644653215010093699)
XLA Ops:
  0.6 75.3 %fused.1 = (bf16[128,2048]{1,0:T(8,128)(2,1)S(1)}, bf16[128,2048]{1,0:T(8,128)(2,1)S(1)}) custom-call(bf16[128,2048]{1,0:T(8,128)(2,1)} %mixer_tokens.1, bf16[2048]{0:T(1024)(128)(2,1)} %mixer_gain.1, bf16[2048,512]{1,0:T(8,128)(2,1)} %in_weight.1, bf16[1,512,512]{2,1,0:T(8,128)(2,1)} %group_weight.1, bf16[512]{0:T(512)(128)(2,1)} %channel_scale.1, ...), custom_call_target="tpu_custom_call" | custom-call | tf_op jit(solution)/shard_map/fused/pallas_call | solution.py:988
  76.0 0.8 %copy.17 = bf16[128,2048]{1,0:T(8,128)(2,1)} copy(bf16[128,2048]{1,0:T(8,128)(2,1)S(1)} %get-tuple-element.2) | data formatting | bytes 1048576
  76.8 0.8 %copy.18 = bf16[128,2048]{1,0:T(8,128)(2,1)} copy(bf16[128,2048]{1,0:T(8,128)(2,1)S(1)} %get-tuple-element.3) | data formatting | bytes 1048576
